TPU v7x, 256 devices: a whole 4x4x8 slice. The times are simulated.
256 devices in a mesh: dp: 4 (over y), kv: 32 (over z, x), tp: 2 (over core).
Axes of the slice: x: 4, y: 4, z: 8, core: 2. Of those that a mesh axis runs over, the one named last changes fastest.
Arguments:
- tokens: bfloat16 [256, 4096], P('dp', ('kv', 'tp')), as said below
- query_weight: bfloat16 [4096, 16, 128], P(None, 'tp', 'kv'), may hold values from -0.09375 to 0.09375
- key_weight: bfloat16 [4096, 16, 128], P(None, 'tp', 'kv'), may hold values from -0.09375 to 0.09375
- value_weight: bfloat16 [4096, 16, 256], P(None, 'tp', 'kv'), may hold values from -0.09375 to 0.09375
- gate_weight: bfloat16 [4096, 16, 256], P(None, 'tp', 'kv'), may hold values from -0.09375 to 0.09375
- decay_weight: bfloat16 [4096, 16, 128], P(None, 'tp', 'kv'), may hold values from -0.09375 to 0.09375
- decay_bias: float32 [16, 128], P('tp'), may hold values from -8 to 2
- states: float32 [256, 16, 128, 256], P(('dp', 'kv'), 'tp'), may hold values from -4 to 4
- head_gain: float32 [16, 256], P('tp'), may hold values from 0.1 to 1.9
- out_weight: bfloat16 [4096, 4096], P(None, ('kv', 'tp')), as said below
- norm1_gain: float32 [4096], P(('kv', 'tp')), may hold values from 0.1 to 1.9
- norm1_bias: float32 [4096], P(('kv', 'tp')), may hold values from -3 to 3
- up_weight: bfloat16 [4096, 16384], P(None, ('kv', 'tp')), may hold values from -0.09375 to 0.09375
- down_weight: bfloat16 [16384, 4096], P(('kv', 'tp')), as said below
- norm2_gain: float32 [4096], P(('kv', 'tp')), may hold values from 0.1 to 1.9
- norm2_bias: float32 [4096], P(('kv', 'tp')), may hold values from -3 to 3
Outputs:
- layer_out: bfloat16 [256, 4096], P('dp', ('kv', 'tp'))
- new_states: float32 [256, 16, 128, 256], P(('dp', 'kv'), 'tp')
Inputs may be any that keep to these rules, and one draw needn't show every extreme that they name: `tokens`: each block of 64 features has its own scale. `out_weight`: entries lie within 13 / sqrt(4096) of zero. `down_weight`: entries lie within 14 / sqrt(16384) of zero.
All inputs are finite; a program needn't handle non-finite values.
Results may differ from a plain program's by a relative error of at most 0.009.
Values may be sent and summed in bfloat16 or wider, within the bound.
A program may use at most 64 MiB of HBM per device.

v0:
```python
import jax
import jax.numpy as jnp
from jax import lax
from jax.sharding import PartitionSpec as P

D = 4096
KEY_DIM = 128


ALPHA = 2.0**0.5
TAU = 16.0
LN_EPS = 1e-05
RMS_EPS = 1e-06


def joined_along(tiles, dim):
    dims = list(tiles.shape[1:])
    dims[dim] *= tiles.shape[0]
    return jnp.moveaxis(tiles, 0, dim).reshape(dims)


def from_everyone(x, axis):
    copies = jnp.broadcast_to(x, (lax.axis_size(axis), *x.shape))
    return lax.all_to_all(copies, axis, split_axis=0, concat_axis=0, tiled=True)


def collect(x, axis, dim):
    return joined_along(from_everyone(x, axis), dim)


def of_everyone(x, axis):
    everything = from_everyone(x, axis)
    return jnp.sum(everything, axis=0)


def in_one(arrays, axis):
    line, at, gathered = (jnp.concatenate([a.reshape(-1) for a in arrays]), 0, [])
    subtotal = of_everyone(line, axis)
    for a in arrays:
        gathered.append(subtotal[at : at + a.size].reshape(a.shape))
        at += a.size
    return tuple(gathered)


def split_up(x, dim, size):
    before, after = (x.shape[:dim], x.shape[dim + 1 :])
    return jnp.moveaxis(x.reshape(*before, size, -1, *after), dim, 0)


def sum_at_owner(x, axis, dim):
    tiles = split_up(x, dim, lax.axis_size(axis))
    arrived = lax.all_to_all(tiles, axis, split_axis=0, concat_axis=0, tiled=True)
    return arrived.astype(jnp.float32).sum(axis=0)


def project_flat(inputs, weight):
    flattened = weight.reshape(weight.shape[0], -1)
    return jnp.dot(inputs, flattened, preferred_element_type=jnp.float32).astype(jnp.bfloat16)


def normalize(inputs, average, spread, row_gain, row_shift):
    return ((inputs - average) * lax.rsqrt(spread + LN_EPS) * row_gain + row_shift).astype(
        jnp.bfloat16
    )


def body(
    tokens,
    query_weight,
    key_weight,
    value_weight,
    gate_weight,
    decay_weight,
    decay_bias,
    states,
    head_gain,
    out_weight,
    norm1_gain,
    norm1_bias,
    up_weight,
    down_weight,
    norm2_gain,
    norm2_bias,
):
    whole = collect(tokens, ("kv", "tp"), 1)
    weights_list = (query_weight, key_weight, decay_weight, value_weight, gate_weight)
    packed = jnp.concatenate([project_flat(whole, weight) for weight in weights_list], axis=1)
    arrived = lax.all_to_all(packed, "kv", split_axis=0, concat_axis=0, tiled=True)
    groups = lax.axis_size("kv")
    seq_count = whole.shape[0] // groups
    local_heads = query_weight.shape[1]
    unpacked = []
    start = 0
    for weight in weights_list:
        channels = weight.shape[2]
        width = local_heads * channels
        block = arrived[:, start : start + width].reshape(groups, seq_count, local_heads, channels)
        block = block.transpose(1, 2, 0, 3).reshape(seq_count, local_heads, groups * channels)
        unpacked.append(block.astype(jnp.float32))
        start = start + width
    query_rows = unpacked[0] * KEY_DIM ** (-0.5)
    key_rows = unpacked[1]
    decay_rows = unpacked[2]
    value_rows = unpacked[3]
    gate_rows = unpacked[4]
    retain = jnp.exp(jax.nn.log_sigmoid(decay_rows + decay_bias) / TAU)
    new_states = retain[..., None] * states + key_rows[..., :, None] * value_rows[..., None, :]
    readout = jnp.einsum("shk,shkv->shv", query_rows, new_states, precision=lax.Precision.HIGHEST)
    readout = (
        readout
        * lax.rsqrt(jnp.mean(readout * readout, axis=-1, keepdims=True) + RMS_EPS)
        * head_gain
    )
    attended = (readout * jax.nn.silu(gate_rows)).astype(jnp.bfloat16)
    seq_count, local_heads, value_width = attended.shape
    flat_width = local_heads * value_width
    collected = collect(attended.reshape(1, seq_count, flat_width), ("kv", "tp"), 0)
    halves = lax.axis_size("tp")
    collected = collected.reshape(-1, halves, seq_count, flat_width)
    columns = out_weight.shape[1]
    out_parts = out_weight.reshape(halves, flat_width, columns)
    mixed_heads = jnp.einsum(
        "atsc,tcd->asd", collected, out_parts, preferred_element_type=jnp.float32
    ).reshape(-1, columns)
    residual_one = ALPHA * tokens.astype(jnp.float32) + mixed_heads
    totals = in_one(
        (
            jnp.sum(residual_one, axis=-1, keepdims=True),
            jnp.sum(residual_one * residual_one, axis=-1, keepdims=True),
        ),
        ("kv", "tp"),
    )
    average = totals[0] / D
    spread = totals[1] / D - average * average
    normed_own = normalize(residual_one, average, spread, norm1_gain, norm1_bias)
    normed = collect(normed_own, ("kv", "tp"), 1)
    lifted = jnp.dot(normed, up_weight, preferred_element_type=jnp.float32)
    hidden = jnp.square(jax.nn.relu(lifted)).astype(jnp.bfloat16)
    mixer_term = jnp.dot(hidden, down_weight, preferred_element_type=jnp.float32)
    share = sum_at_owner(mixer_term.astype(jnp.bfloat16), ("kv", "tp"), 1)
    residual_two = ALPHA * normed_own.astype(jnp.float32) + share
    totals = in_one(
        (
            jnp.sum(residual_two, axis=-1, keepdims=True),
            jnp.sum(residual_two * residual_two, axis=-1, keepdims=True),
        ),
        ("kv", "tp"),
    )
    average = totals[0] / D
    spread = totals[1] / D - average * average
    layer_out = normalize(residual_two, average, spread, norm2_gain, norm2_bias)
    return (layer_out, new_states)


def solution(mesh):
    placed = (
        P("dp", ("kv", "tp")),
        P(None, "tp", "kv"),
        P(None, "tp", "kv"),
        P(None, "tp", "kv"),
        P(None, "tp", "kv"),
        P(None, "tp", "kv"),
        P("tp", None),
        P(("dp", "kv"), "tp", None, None),
        P("tp", None),
        P(None, ("kv", "tp")),
        P(("kv", "tp")),
        P(("kv", "tp")),
        P(None, ("kv", "tp")),
        P(("kv", "tp"), None),
        P(("kv", "tp")),
        P(("kv", "tp")),
    )
    return jax.shard_map(
        body,
        mesh=mesh,
        in_specs=placed,
        out_specs=(P("dp", ("kv", "tp")), P(("dp", "kv"), "tp", None, None)),
        check_vma=False,
    )
```

profile of v0, /device:TPU:1, one launch (start us, length us, event | category | flops | bytes accessed | tf_op | source)
XLA Modules:
  0.0 191.4 jit_solution(319838713563614657)
XLA Ops:
  0.6 1.1 broadcast_in_dim.10
  1.8 1.5 reshape.163
  3.3 13.3 %all-to-all-start = ((bf16[64,2,2048]{2,1,0:T(2,128)(2,1)}), bf16[64,2,2048]{2,1,0:T(2,128)(2,1)}, u32[]{:S(2)}, u32[]{:S(2)}) async-start(bf16[64,2,2048]{2,1,0:T(2,128)(2,1)} %reshape.163), calls=%async_computation | async-start | bytes 1048576 | tf_op jit(solution)/shard_map/all_to_all | solution.py:24
  16.6 1.0 reshape.143
  17.6 1.7 reshape.144
  19.4 0.8 reshape.145
  20.1 14.1 %all-to-all-done = bf16[64,2,2048]{2,1,0:T(2,128)(2,1)} async-done(((bf16[64,2,2048]{2,1,0:T(2,128)(2,1)}), bf16[64,2,2048]{2,1,0:T(2,128)(2,1)}, u32[]{:S(2)}, u32[]{:S(2)}) %all-to-all-start) | async-done | bytes 524320 | tf_op jit(solution)/shard_map/all_to_all | solution.py:24
  34.2 2.3 %reshape.164 = bf16[64,64,64]{2,1,0:T(8,128)(2,1)S(1)} reshape(bf16[64,2,2048]{2,1,0:T(2,128)(2,1)} %all-to-all-done) | data formatting | bytes 1048576
  36.5 1.6 copy.110
  38.2 2.1 %reshape.142 = bf16[64,4096]{1,0:T(8,128)(2,1)S(1)} reshape(bf16[64,64,64]{2,1,0:T(8,128)(2,1)} %copy.110) | data formatting | bytes 1048576 | tf_op jit(solution)/shard_map/reshape | solution.py:19
  40.3 1.2 convolution_convert_fusion.3
  41.5 0.3 convolution_convert_fusion.4
  41.8 0.3 convolution_convert_fusion.5
  42.0 0.1 copy.111
  42.1 0.1 copy.112
  42.3 0.1 copy.113
  42.4 1.3 convolution_convert_fusion.1
  43.7 1.3 convolution_convert_fusion.2
  45.0 0.1 concatenate.9
  45.2 13.0 %all_to_all.44 = bf16[32,2,224]{2,1,0:T(2,128)(2,1)S(1)} all-to-all(bf16[32,2,224]{2,1,0:T(2,128)(2,1)S(1)} %all_to_all.29), channel_id=1, replica_groups=mesh['dp'=4,'kv'=32,'tp'=2] {'kv'}, dimensions={0} | all-to-all | bytes 57344 | tf_op jit(solution)/shard_map/all_to_all | solution.py:88
  58.2 0.1 slice_convert_fusion.1
  58.4 0.1 reshape.156
  58.5 0.5 copy.115
  59.0 0.1 reshape.158
  59.2 0.1 copy.119
  59.3 0.2 reshape.154
  59.4 0.1 mul.117
  59.6 0.5 copy.114
  60.1 0.1 reshape.157
  60.2 0.5 copy.117
  60.7 0.1 reshape.159
  60.9 0.1 copy.120
  61.0 0.2 reshape.155
  61.2 1.9 %multiply_add_fusion = f32[2,8,128,256]{3,2,1,0:T(8,128)S(1)} fusion(f32[2,8,128,256]{3,2,1,0:T(8,128)} %param.23, f32[2,8,256]{2,1,0:T(8,128)S(1)} %reshape.154, f32[2,8,128]{2,1,0:T(8,128)S(1)} %copy.118, f32[2,8,128]{2,1,0:T(8,128)S(1)} %fusion.15), kind=kLoop, calls=%fused_computation.2 | loop fusion | flops 1572864 | bytes 4227072 | tf_op jit(solution)/shard_map/add | solution.py:107
  63.1 1.3 copy-done.1
  64.4 1.1 fusion.19
  65.6 0.1 fusion.8
  65.7 1.1 broadcast_in_dim.11
  66.8 6.4 %all-to-all-start.2 = ((bf16[64,1,2,2048]{3,2,1,0:T(2,128)(2,1)}), bf16[64,1,2,2048]{3,2,1,0:T(2,128)(2,1)S(1)}, u32[]{:S(2)}, u32[]{:S(2)}) async-start(bf16[64,1,2,2048]{3,2,1,0:T(2,128)(2,1)} %broadcast_in_dim.11), calls=%async_computation.2 | async-start | bytes 1048576 | tf_op jit(solution)/shard_map/all_to_all | solution.py:24
  73.2 0.1 copy.109
  73.3 17.7 %all-to-all-done.2 = bf16[64,1,2,2048]{3,2,1,0:T(2,128)(2,1)S(1)} async-done(((bf16[64,1,2,2048]{3,2,1,0:T(2,128)(2,1)}), bf16[64,1,2,2048]{3,2,1,0:T(2,128)(2,1)S(1)}, u32[]{:S(2)}, u32[]{:S(2)}) %all-to-all-start.2) | async-done | bytes 524320 | tf_op jit(solution)/shard_map/all_to_all | solution.py:24
  91.0 0.4 copy.121
  91.4 0.2 dot_general.38
  91.6 1.3 fusion.18
  93.0 15.1 %all_to_all.45 = f32[64,1,128]{2,1,0:T(1,128)S(1)} all-to-all(f32[64,1,128]{2,1,0:T(1,128)S(1)} %broadcast_in_dim.12), channel_id=1, replica_groups=mesh['dp'=4,'kv'=32,'tp'=2] {'kv','tp'}, dimensions={0} | all-to-all | bytes 65536 | tf_op jit(solution)/shard_map/all_to_all | solution.py:24
  108.2 0.1 add_convert_fusion.1
  108.3 0.1 copy.124
  108.4 0.3 broadcast_in_dim.13
  108.7 1.5 reshape.165
  110.2 23.3 %all_to_all.46 = bf16[64,2,2048]{2,1,0:T(2,128)(2,1)} all-to-all(bf16[64,2,2048]{2,1,0:T(2,128)(2,1)} %reshape.165), channel_id=1, replica_groups=mesh['dp'=4,'kv'=32,'tp'=2] {'kv','tp'}, dimensions={0} | all-to-all | bytes 1048576 | tf_op jit(solution)/shard_map/all_to_all | solution.py:24
  133.5 2.3 %reshape.166 = bf16[64,64,64]{2,1,0:T(8,128)(2,1)S(1)} reshape(bf16[64,2,2048]{2,1,0:T(2,128)(2,1)} %all_to_all.46) | data formatting | bytes 1048576
  135.8 1.7 copy.125
  137.5 2.1 %reshape.150 = bf16[64,4096]{1,0:T(8,128)(2,1)S(1)} reshape(bf16[64,64,64]{2,1,0:T(8,128)(2,1)} %copy.125) | data formatting | bytes 1048576 | tf_op jit(solution)/shard_map/reshape | solution.py:19
  139.5 3.8 %convolution_convert_fusion = bf16[64,4096]{1,0:T(8,128)(2,1)} fusion(bf16[256,4096]{1,0:T(8,128)(2,1)S(1)} %copy-done, bf16[64,4096]{1,0:T(8,128)(2,1)S(1)} %reshape.150, bf16[4096,256]{1,0:T(8,128)(2,1)} %param.28), kind=kOutput, calls=%fused_computation | convolution fusion | flops 268746752 | bytes 5242880 | tf_op jit(solution)/shard_map/dot_general | solution.py:139
  143.3 2.1 %reshape.151 = bf16[64,64,64]{2,1,0:T(8,128)(2,1)S(1)} reshape(bf16[64,4096]{1,0:T(8,128)(2,1)} %convolution_convert_fusion) | data formatting | bytes 1048576 | tf_op jit(solution)/shard_map/reshape | solution.py:47
  145.4 1.7 copy.147
  147.1 2.3 %reshape.167 = bf16[64,2,2048]{2,1,0:T(2,128)(2,1)S(1)} reshape(bf16[64,64,64]{2,1,0:T(8,128)(2,1)} %bitcast.80) | data formatting | bytes 1048576
  149.4 23.3 %all_to_all.47 = bf16[64,2,2048]{2,1,0:T(2,128)(2,1)} all-to-all(bf16[64,2,2048]{2,1,0:T(2,128)(2,1)S(1)} %reshape.167), channel_id=1, replica_groups=mesh['dp'=4,'kv'=32,'tp'=2] {'kv','tp'}, dimensions={0} | all-to-all | bytes 1048576 | tf_op jit(solution)/shard_map/all_to_all | solution.py:52
  172.7 2.3 %reshape.168 = bf16[64,64,64]{2,1,0:T(8,128)(2,1)S(1)} reshape(bf16[64,2,2048]{2,1,0:T(2,128)(2,1)} %all_to_all.47) | data formatting | bytes 1048576
  175.0 0.2 convert_reduce_fusion
  175.3 0.1 fusion.12
  175.5 14.9 %all_to_all.48 = f32[64,1,128]{2,1,0:T(1,128)S(1)} all-to-all(f32[64,1,128]{2,1,0:T(1,128)S(1)} %broadcast_in_dim.14), channel_id=1, replica_groups=mesh['dp'=4,'kv'=32,'tp'=2] {'kv','tp'}, dimensions={0} | all-to-all | bytes 65536 | tf_op jit(solution)/shard_map/all_to_all | solution.py:24
  190.6 0.1 add_convert_fusion
  190.7 0.7 copy.130
  (41 shorter events, 1.0 us)
Async XLA Ops:
  0.6 138.9 %copy-start = (bf16[256,4096]{1,0:T(8,128)(2,1)S(1)}, bf16[256,4096]{1,0:T(8,128)(2,1)}, u32[]{:S(2)}) copy-start(bf16[256,4096]{1,0:T(8,128)(2,1)} %param.29) | copy-start | bytes 6291460
  3.3 16.0 %copy-start.3 = (bf16[4096,8,4]{0,2,1:T(4,128)(2,1)S(1)}, bf16[4096,8,4]{0,2,1:T(4,128)(2,1)}, u32[]{:S(2)}) copy-start(bf16[4096,8,4]{0,2,1:T(4,128)(2,1)} %param.21) | copy-start | bytes 786436
  3.3 30.9 %all-to-all-start = ((bf16[64,2,2048]{2,1,0:T(2,128)(2,1)}), bf16[64,2,2048]{2,1,0:T(2,128)(2,1)}, u32[]{:S(2)}, u32[]{:S(2)}) async-start(bf16[64,2,2048]{2,1,0:T(2,128)(2,1)} %reshape.163), calls=%async_computation | async-start | bytes 1048576 | tf_op jit(solution)/shard_map/all_to_all | solution.py:24
  38.2 3.3 %copy-start.2 = (bf16[4096,32]{0,1:T(8,128)(2,1)S(1)}, bf16[4096,32]{0,1:T(8,128)(2,1)}, u32[]{:S(2)}) copy-start(bf16[4096,32]{0,1:T(8,128)(2,1)} %reshape.144) | copy-start | bytes 786436
  59.0 2.2 %copy-start.8 = (f32[8,128]{1,0:T(8,128)S(1)}, f32[8,128]{1,0:T(8,128)}, u32[]{:S(2)}) copy-start(f32[8,128]{1,0:T(8,128)} %param.22) | copy-start | bytes 12292
  63.1 1.3 copy-start.1
  64.4 1.2 copy-start.5
  64.4 8.8 %copy-start.4 = (bf16[64,64]{1,0:T(8,128)(2,1)S(1)}, bf16[64,64]{1,0:T(8,128)(2,1)}, u32[]{:S(2)}) copy-start(bf16[64,64]{1,0:T(8,128)(2,1)} %param.16) | copy-start | bytes 24580
  66.8 41.4 %copy-start.6 = (f32[64]{0:T(128)S(1)}, f32[64]{0:T(128)}, u32[]{:S(2)}) copy-start(f32[64]{0:T(128)} %param.27) | copy-start | bytes 772
  66.8 41.4 %copy-start.7 = (f32[64]{0:T(128)S(1)}, f32[64]{0:T(128)}, u32[]{:S(2)}) copy-start(f32[64]{0:T(128)} %param.26) | copy-start | bytes 772
  66.8 24.2 %all-to-all-start.2 = ((bf16[64,1,2,2048]{3,2,1,0:T(2,128)(2,1)}), bf16[64,1,2,2048]{3,2,1,0:T(2,128)(2,1)S(1)}, u32[]{:S(2)}, u32[]{:S(2)}) async-start(bf16[64,1,2,2048]{3,2,1,0:T(2,128)(2,1)} %broadcast_in_dim.11), calls=%async_computation.2 | async-start | bytes 1048576 | tf_op jit(solution)/shard_map/all_to_all | solution.py:24
  149.4 41.1 %copy-start.9 = (f32[64]{0:T(128)S(1)}, f32[64]{0:T(128)}, u32[]{:S(2)}) copy-start(f32[64]{0:T(128)} %param.31) | copy-start | bytes 772
  149.4 41.1 %copy-start.10 = (f32[64]{0:T(128)S(1)}, f32[64]{0:T(128)}, u32[]{:S(2)}) copy-start(f32[64]{0:T(128)} %param.30) | copy-start | bytes 772
where the time goes:
time: 192 us; the launch traced here: 191 us
  blocking collectives  89.5 us (47%)
  local copies, waits for them, and re-layouts  35.5 us (18%)
  waiting for transfers between devices  31.8 us (17%)
  starting transfers between devices  19.7 us (10%)
  matrix products  10.6 us (6%)
  other arithmetic  3.19 us (2%)
    all_to_all x3, blocking collectives, from_everyone(): return lax.all_to_all(copies, axis, split_axis=0, concat_axis=0, tiled=True)  53.3 us
    all_to_all x2, waiting for transfers between devices, from_everyone(): return lax.all_to_all(copies, axis, split_axis=0, concat_axis=0, tiled=True)  31.8 us
    all_to_all x1, blocking collectives, sum_at_owner(): lax.all_to_all(tiles, axis, split_axis=0, concat_axis=0, tiled=True)  23.3 us
    all_to_all x2, starting transfers between devices, from_everyone(): return lax.all_to_all(copies, axis, split_axis=0, concat_axis=0, tiled=True)  19.7 us
    unnamed x31, local copies, waits for them, and re-layouts  14.5 us
    all_to_all x1, blocking collectives, body(): lax.all_to_all(packed, 'kv', split_axis=0, concat_axis=0, tiled=True)  13 us
    dot_general x5, matrix products, project_flat(): jnp.dot(inputs, flattened, preferred_element_type=jnp.float32)  4.4 us
    reshape x2, local copies, waits for them, and re-layouts, joined_along(): return jnp.moveaxis(tiles, 0, dim).reshape(dims)  4.16 us
  transfers between devices with their start and end apart: 2, of which 2 were waited for; matrix products, arithmetic and copies ran while one was open for 2% of the time, Pallas kernels for 0%

commit v1 on v0

v1 whole, which is shorter than its diff:
```python
import functools

import jax
import jax.numpy as jnp
from jax import lax
from jax.experimental import pallas as pl
from jax.experimental.pallas import tpu as pltpu
from jax.sharding import PartitionSpec as P

D = 4096
KEY_DIM = 128
ALPHA = 2.0**0.5
TAU = 16.0
LN_EPS = 1e-05
RMS_EPS = 1e-06
MESH = pl.DeviceIdType.MESH
F32 = jnp.float32
BF16 = jnp.bfloat16
NT = (((1,), (1,)), ((), ()))
NN = (((1,), (0,)), ((), ()))
TN = (((0,), (0,)), ((), ()))
CHIPS = 32


def dot(a, b, dims):
    return lax.dot_general(a, b, dims, preferred_element_type=F32)


def iota(shape, dim):
    return lax.broadcasted_iota(jnp.int32, shape, dim)


def kernel(
    tok, wq, wk, wd, wv, wg, bias, states, head_gain, ow, g1, b1, up, dn, g2, b2,
    out, new_states,
    wst, wc, owc, upc, dnc, st,
    s_a, r_a, s_g, r_g, x, s_b, r_b, ro, s_c, r_c, att32, att,
    s_e, r_e, s_m, r_m, xt, xn, s_y, r_y, s_h, r_h, s_f, r_f, sq,
    own_sem, w_send, w_recv, st_out_sem,
    a_sem, g_sem, b_sem, c_sem, e_sem, m_sem, y_sem, h_sem, f_sem,
):
    kv = lax.axis_index("kv")
    t = lax.axis_index("tp")
    z, xx = kv // 4, kv % 4
    half = kv // 16
    mine = half == t

    def chip_at(j):
        i = j // 4
        dz = lax.rem(4 + ((i + 1) // 2) * (2 * lax.rem(i, 2) - 1) + 8, 8)
        dx = lax.rem(j + 1, 4)
        return lax.rem(z + dz, 8) * 4 + lax.rem(xx + dx, 4)

    def rcopy(src, dst, sems, kv_to, t_to):
        return pltpu.make_async_remote_copy(
            src_ref=src, dst_ref=dst, send_sem=sems.at[0], recv_sem=sems.at[1],
            device_id={"kv": kv_to, "tp": t_to}, device_id_type=MESH,
        )

    def drain(ref, sem):
        pltpu.make_async_copy(ref, ref, sem).wait()

    own = [
        pltpu.make_async_copy(wq, wst.at[t, 0], own_sem.at[0]),
        pltpu.make_async_copy(wk, wst.at[t, 1], own_sem.at[1]),
        pltpu.make_async_copy(wd, wst.at[t, 2], own_sem.at[2]),
        pltpu.make_async_copy(wv, wc.at[t, pl.ds(96, 64)], own_sem.at[3]),
        pltpu.make_async_copy(wg, wc.at[t, pl.ds(160, 64)], own_sem.at[4]),
        pltpu.make_async_copy(states, st, own_sem.at[5]),
        pltpu.make_async_copy(ow, owc.at[t], own_sem.at[6]),
        pltpu.make_async_copy(up, upc.at[t], own_sem.at[7]),
        pltpu.make_async_copy(dn, dnc.at[t], own_sem.at[8]),
    ]
    for c in own:
        c.start()

    barrier = pltpu.get_barrier_semaphore()

    @pl.loop(1, 64)
    def _(i):
        p = lax.rem(kv * 2 + t + i, 64)
        pl.semaphore_signal(barrier, inc=1, device_id={"kv": p // 2, "tp": lax.rem(p, 2)}, device_id_type=MESH)

    tk = tok[...].astype(F32)
    for hh in range(2):
        s_a[hh] = jnp.concatenate(
            [tk[32 * hh : 32 * hh + 16], tk[32 * hh + 16 : 32 * hh + 32]], axis=1
        ).astype(BF16)
    s_g[0:1] = jnp.concatenate([g1[...], b1[...]], axis=1)
    s_g[1:2] = jnp.concatenate([g2[...], b2[...]], axis=1)
    me = t * CHIPS + kv
    r_a[me] = s_a[t]
    r_g[me] = s_g[...]
    pl.semaphore_wait(barrier, 63)

    @pl.loop(0, CHIPS)
    def _(j):
        kp = chip_at(j)
        for tt in range(2):

            @pl.when(jnp.logical_or(kp != kv, t != tt))
            def _():
                rcopy(s_a.at[tt], r_a.at[me], a_sem, kp, tt).start()

    partner = 1 - t

    def wcopy(src, dst, i):
        return pltpu.make_async_remote_copy(
            src_ref=src, dst_ref=dst, send_sem=w_send.at[i], recv_sem=w_recv.at[i],
            device_id={"kv": kv, "tp": partner}, device_id_type=MESH,
        )

    wcopies = [
        wcopy(wq, wst.at[t, 0], 0),
        wcopy(wk, wst.at[t, 1], 1),
        wcopy(wd, wst.at[t, 2], 2),
        wcopy(wv, wc.at[t, pl.ds(96, 64)], 3),
        wcopy(wg, wc.at[t, pl.ds(160, 64)], 4),
        wcopy(ow, owc.at[t], 5),
        wcopy(up, upc.at[t], 6),
        wcopy(dn, dnc.at[t], 7),
    ]
    for c in wcopies[:5]:
        c.start()

    @pl.loop(0, CHIPS)
    def _(j):
        kp = chip_at(j)
        for tt in range(2):

            @pl.when(jnp.logical_or(kp != kv, t != tt))
            def _():
                rcopy(s_g, r_g.at[me], g_sem, kp, tt).start()

    lane = iota((16, 128), 1) < 64
    col = iota((224, 256), 1)
    row = iota((224, 256), 0)
    low = col < 128
    j2 = col - 128
    src_low = ((col % 32) // 8) * 32 + (col % 8) * 4 + col // 32
    src_high = 96 + ((j2 % 16) // 8) * 64 + (j2 % 8) * 8 + j2 // 16
    src_low = jnp.where(col % 32 < 24, src_low, -1)
    perm = jnp.where(row == jnp.where(low, src_low, src_high), 1.0, 0.0).astype(BF16)
    e1 = jnp.where(iota((128, 128), 1) == (iota((128, 128), 0) % 4) * 32 + iota((128, 128), 0) // 4, 1.0, 0.0).astype(BF16)
    e2 = jnp.where(iota((256, 256), 0) == (iota((256, 256), 1) % 8) * 32 + iota((256, 256), 1) // 8, 1.0, 0.0).astype(BF16)
    zero = lambda n: jnp.zeros((n, 128), F32)
    bias_full = jnp.concatenate(
        [zero(16), bias[...], zero(24), bias[...], zero(8 + 64)], axis=0
    ).T[:, :64]

    for c in own:
        c.wait()
    for c in wcopies[:5]:
        c.wait()
    for c in wcopies[5:]:
        c.start()
    for tt in range(2):
        for ty in range(3):
            for h in range(0, 8, 4):
                wc[tt, ty * 32 + h * 4 : ty * 32 + h * 4 + 16, :] = jnp.concatenate(
                    [wst[tt, ty, h + i].astype(F32) for i in range(4)], axis=0
                ).astype(BF16)

    drain(r_a.at[pl.ds(0, 63)], a_sem.at[1])
    for c in range(CHIPS):
        a0 = r_a[c].astype(F32)
        a1 = r_a[CHIPS + c].astype(F32)
        x[0:16, c * 128 : (c + 1) * 128] = jnp.where(lane, a0, pltpu.roll(a1, 64, 1)).astype(BF16)
        x[16:32, c * 128 : (c + 1) * 128] = jnp.where(lane, pltpu.roll(a0, 64, 1), a1).astype(BF16)

    for tt in range(2):
        p = dot(x[...], wc[tt], NT).astype(BF16)
        p = dot(p, perm, NN)
        for i in range(16):
            s_b[i, tt] = p[2 * i : 2 * i + 2, :]

    @pl.loop(0, 16)
    def _(i):
        k16 = lax.rem(kv + 8 + i, 16)
        kp = 16 * t + k16
        for tt in range(2):

            @pl.when(jnp.logical_or(kp != kv, t != tt))
            def _():
                rcopy(s_b.at[k16, tt], r_b.at[kv], b_sem, kp, tt).start()

    @pl.when(mine)
    def _():
        r_b[kv] = s_b[lax.rem(kv, 16), t]
        drain(r_b.at[pl.ds(0, 31)], b_sem.at[1])

    @pl.when(jnp.logical_not(mine))
    def _():
        drain(r_b, b_sem.at[1])

    qkd, vg = [], []
    for s in range(2):
        rs = r_b[:, s, :]
        qkd.append(jnp.concatenate([rs[:, c * 32 : (c + 1) * 32] for c in range(4)], axis=0))
        vg.append(jnp.concatenate([rs[:, 128 + c * 16 : 144 + c * 16] for c in range(8)], axis=0))
    cols = dot(e1, jnp.concatenate(qkd, axis=1).astype(BF16), NN)
    rows = [dot(v.astype(BF16), e2, TN) for v in vg]
    decay = cols + bias_full
    log_sig = jnp.minimum(decay, 0.0) - jnp.log1p(jnp.exp(-jnp.abs(decay)))
    retain = jnp.exp(log_sig / TAU)
    q = cols * KEY_DIM ** (-0.5)
    for s in range(2):
        for h in range(8):
            o = s * 32 + h
            new = retain[:, o + 16 : o + 17] * st[s, h] + cols[:, o + 8 : o + 9] * rows[s][h : h + 1, :]
            st[s, h] = new
            ro[s * 8 + h : s * 8 + h + 1, :] = jnp.sum(q[:, o : o + 1] * new, axis=0, keepdims=True)
    st_out = pltpu.make_async_copy(st, new_states, st_out_sem)
    st_out.start()
    readout = ro[...]
    gate = jnp.concatenate([rows[0][8:16], rows[1][8:16]], axis=0)
    hg = jnp.concatenate([head_gain[...], head_gain[...]], axis=0)
    readout = readout * lax.rsqrt(jnp.mean(readout * readout, axis=-1, keepdims=True) + RMS_EPS) * hg
    s_c[...] = (readout * (gate / (1.0 + jnp.exp(-gate)))).astype(BF16)

    slot_c = t * 16 + lax.rem(kv, 16)

    @pl.loop(0, CHIPS)
    def _(j):
        kp = chip_at(j)

        @pl.when(jnp.logical_or(kp != kv, t != half))
        def _():
            rcopy(s_c, r_c.at[slot_c], c_sem, kp, half).start()

    @pl.when(mine)
    def _():
        r_c[slot_c] = s_c[...]
        drain(r_c.at[pl.ds(0, 31)], c_sem.at[1])

    @pl.when(jnp.logical_not(mine))
    def _():
        drain(r_c, c_sem.at[1])

    for tt in range(2):
        arrived = r_c[tt * 16 : (tt + 1) * 16].astype(F32).reshape(256, 256)
        for n in range(2):
            att32[n] = arrived[:, n * 128 : (n + 1) * 128]
            for h in range(8):
                at = tt * 2048 + h * 256 + n * 128
                att[:, at : at + 128] = att32[n, pl.ds(h, 32, stride=8), :].astype(BF16)
    wcopies[5].wait()
    mixed = jnp.concatenate([dot(att[...], owc[tt], NT) for tt in range(2)], axis=1)
    at_chip = pl.multiple_of(kv * 128, 128)
    res1 = ALPHA * x[:, pl.ds(at_chip, 128)].astype(F32) + mixed

    m_own = jnp.mean(res1, axis=-1, keepdims=True)
    sq[0:32, :] = jnp.broadcast_to(m_own, (32, 128))
    sq[32:128, :] = jnp.zeros((96, 128), F32)
    s_m[...] = sq[...].T[0:1, :]
    s_e[...] = (res1 - m_own).astype(BF16)

    @pl.loop(0, CHIPS - 1)
    def _(j):
        kp = chip_at(j)
        rcopy(s_e, r_e.at[kv], e_sem, kp, t).start()
        rcopy(s_m, r_m.at[kv], m_sem, kp, t).start()

    r_e[kv] = s_e[...]
    r_m[kv] = s_m[...]
    drain(r_g.at[pl.ds(0, 63)], g_sem.at[1])
    ga = r_g[0:32, 0, :]
    gb = r_g[32:64, 0, :]
    lane32 = iota((32, 128), 1) < 64
    gain1 = jnp.where(lane32, ga, pltpu.roll(gb, 64, 1))
    bias1 = jnp.where(lane32, pltpu.roll(ga, 64, 1), gb)
    wcopies[6].wait()
    wcopies[7].wait()
    drain(r_m.at[pl.ds(0, 31)], m_sem.at[1])
    drain(r_e.at[pl.ds(0, 31)], e_sem.at[1])
    sq[0:32, :] = r_m[:, 0, :]
    means = sq[...].T[0:32, 0:32]
    acc = jnp.zeros((32, 128), F32)
    for c in range(CHIPS):
        acc = acc + r_e[c].astype(F32)
    mean = (jnp.sum(acc, axis=-1, keepdims=True) + 128.0 * jnp.sum(means, axis=-1, keepdims=True)) / D
    acc = jnp.zeros((32, 128), F32)
    for c in range(CHIPS):
        v = r_e[c].astype(F32) + (means[:, c : c + 1] - mean)
        xt[c] = v
        acc = acc + v * v
    inv = lax.rsqrt(jnp.sum(acc, axis=-1, keepdims=True) / D + LN_EPS)
    for c in range(CHIPS):
        xn[:, c * 128 : (c + 1) * 128] = (xt[c] * inv * gain1[c : c + 1, :] + bias1[c : c + 1, :]).astype(BF16)

    hidden = []
    for tt in range(2):
        lifted = jnp.maximum(dot(xn[...], upc[tt], NN), 0.0)
        hidden.append((lifted * lifted).astype(BF16))

    @pl.loop(0, CHIPS)
    def _(j):
        kp = chip_at(j)
        cl = pl.ds(pl.multiple_of(kp * 128, 128), 128)
        y = dot(hidden[0], dnc[0, :, cl], NN) + dot(hidden[1], dnc[1, :, cl], NN)
        s_y[kp] = y.astype(BF16)

        @pl.when(kp != kv)
        def _():
            rcopy(s_y.at[kp], r_y.at[kv], y_sem, kp, t).start()

    r_y[kv] = s_y[kv]
    drain(r_y.at[pl.ds(0, 31)], y_sem.at[1])
    res2 = ALPHA * xn[:, pl.ds(at_chip, 128)].astype(F32)
    for c in range(CHIPS):
        res2 = res2 + r_y[c].astype(F32)

    m_own = jnp.mean(res2, axis=-1, keepdims=True)
    dev = res2 - m_own
    v_own = jnp.sum(dev * dev, axis=-1, keepdims=True)
    sq[0:32, :] = jnp.where(iota((32, 128), 1) == 0, m_own, v_own)
    s_h[...] = sq[...].T[0:2, :]

    @pl.loop(0, CHIPS - 1)
    def _(j):
        rcopy(s_h, r_h.at[kv], h_sem, chip_at(j), t).start()

    r_h[kv] = s_h[...]
    drain(r_h.at[pl.ds(0, 31)], h_sem.at[1])
    ms = r_h[:, 0, :]
    vs = r_h[:, 1, :]
    mean = jnp.mean(ms, axis=0, keepdims=True)
    dm = ms - mean
    spread = (jnp.sum(vs, axis=0, keepdims=True) + 128.0 * jnp.sum(dm * dm, axis=0, keepdims=True)) / D
    inv = lax.rsqrt(spread + LN_EPS)
    sq[0:1, :] = mean
    sq[1:2, :] = inv
    back = sq[...].T
    own0 = r_g[kv][1:2, :]
    own1 = r_g[CHIPS + kv][1:2, :]
    lane1 = iota((1, 128), 1) < 64
    gain2 = jnp.where(lane1, own0, pltpu.roll(own1, 64, 1))
    bias2 = jnp.where(lane1, pltpu.roll(own0, 64, 1), own1)
    o = ((res2 - back[0:32, 0:1]) * back[0:32, 1:2] * gain2 + bias2)
    s_f[...] = o.astype(BF16)
    last = rcopy(s_f, r_f, f_sem, kv, partner)
    last.start()
    first = t == 0
    out[pl.ds(pl.multiple_of(t * 32, 32), 32), :] = jnp.where(first, o, pltpu.roll(o, 64, 1))[:, :64].astype(BF16)
    last.wait()
    f = r_f[...].astype(F32)
    out[pl.ds(pl.multiple_of(partner * 32, 32), 32), :] = jnp.where(first, f, pltpu.roll(f, 64, 1))[:, :64].astype(BF16)

    drain(r_a.at[pl.ds(0, 63)], a_sem.at[0])
    drain(r_g.at[pl.ds(0, 63)], g_sem.at[0])

    @pl.when(mine)
    def _():
        drain(r_b.at[pl.ds(0, 31)], b_sem.at[0])
        drain(r_c.at[pl.ds(0, 31)], c_sem.at[0])

    @pl.when(jnp.logical_not(mine))
    def _():
        drain(r_b, b_sem.at[0])
        drain(r_c, c_sem.at[0])

    drain(r_e.at[pl.ds(0, 31)], e_sem.at[0])
    drain(r_m.at[pl.ds(0, 31)], m_sem.at[0])
    drain(r_y.at[pl.ds(0, 31)], y_sem.at[0])
    drain(r_h.at[pl.ds(0, 31)], h_sem.at[0])
    st_out.wait()


def body(
    tokens, query_weight, key_weight, value_weight, gate_weight, decay_weight, decay_bias, states,
    head_gain, out_weight, norm1_gain, norm1_bias, up_weight, down_weight, norm2_gain, norm2_bias,
):
    flip = lambda w: w.transpose(1, 2, 0)
    flat = lambda w: flip(w).reshape(-1, D)
    line = lambda v: v.reshape(1, -1)
    vmem = pl.BlockSpec(memory_space=pltpu.VMEM)
    hbm = pl.BlockSpec(memory_space=pl.ANY)
    V = pltpu.VMEM
    dma = pltpu.SemaphoreType.DMA
    scratch = [
        V((2, 3, 8, 4, D), BF16),
        V((2, 224, D), BF16),
        V((2, 64, D), BF16),
        V((2, D, 256), BF16),
        V((2, 256, D), BF16),
        V((2, 8, 128, 256), F32),
        V((2, 16, 128), BF16), V((64, 16, 128), BF16),
        V((2, 128), F32), V((64, 2, 128), F32),
        V((32, D), BF16),
        V((16, 2, 2, 256), F32), V((32, 2, 256), F32),
        V((16, 256), F32),
        V((16, 256), BF16), V((32, 16, 256), BF16),
        V((2, 256, 128), F32), V((32, D), BF16),
        V((32, 128), BF16), V((32, 32, 128), BF16),
        V((1, 128), F32), V((32, 1, 128), F32),
        V((32, 32, 128), F32), V((32, D), BF16),
        V((32, 32, 128), BF16), V((32, 32, 128), BF16),
        V((2, 128), F32), V((32, 2, 128), F32),
        V((32, 128), BF16), V((32, 128), BF16),
        V((128, 128), F32),
        dma((9,)), dma((8,)), dma((8,)), dma,
    ] + [dma((2,))] * 9
    return pl.pallas_call(
        kernel,
        out_shape=(
            jax.ShapeDtypeStruct((64, 64), BF16),
            jax.ShapeDtypeStruct((2, 8, 128, 256), F32),
        ),
        in_specs=[vmem] + [hbm] * 5 + [vmem, hbm, vmem, hbm, vmem, vmem, hbm, hbm, vmem, vmem],
        out_specs=(vmem, hbm),
        scratch_shapes=scratch,
        compiler_params=pltpu.CompilerParams(
            collective_id=0, has_side_effects=True, vmem_limit_bytes=60 * 1024 * 1024
        ),
        name="layer_step",
    )(
        tokens, flip(query_weight), flip(key_weight), flip(decay_weight), flat(value_weight), flat(gate_weight),
        decay_bias, states, head_gain, out_weight.T, line(norm1_gain), line(norm1_bias), up_weight, down_weight,
        line(norm2_gain), line(norm2_bias),
    )


def solution(mesh):
    placed = (
        P("dp", ("kv", "tp")),
        P(None, "tp", "kv"),
        P(None, "tp", "kv"),
        P(None, "tp", "kv"),
        P(None, "tp", "kv"),
        P(None, "tp", "kv"),
        P("tp", None),
        P(("dp", "kv"), "tp", None, None),
        P("tp", None),
        P(None, ("kv", "tp")),
        P(("kv", "tp")),
        P(("kv", "tp")),
        P(None, ("kv", "tp")),
        P(("kv", "tp"), None),
        P(("kv", "tp")),
        P(("kv", "tp")),
    )
    return jax.shard_map(
        body,
        mesh=mesh,
        in_specs=placed,
        out_specs=(P("dp", ("kv", "tp")), P(("dp", "kv"), "tp", None, None)),
        check_vma=False,
    )
```

time: 192 us -> 73.4 us (0.38)
  blocking collectives: 89.5 us -> 0 us
  Pallas kernels: 0 us -> 68.1 us
  waiting for transfers between devices: 31.8 us -> 0 us
  local copies, waits for them, and re-layouts: 35.5 us -> 4.42 us
  starting transfers between devices: 19.7 us -> 0 us
  matrix products: 10.6 us -> 0 us
  other arithmetic: 3.19 us -> 0 us
    all_to_all x5 -> x0, blocking collectives: 89.5 us -> none  [the longest x3 53.3 us: from_everyone(): return lax.all_to_all(copies, axis, split_axis=0, concat_axis=0, tiled=True)]
    pallas_call x0 -> x1, Pallas kernels: none -> 68.1 us  [body(): pl.pallas_call(kernel, out_shape=(jax.ShapeDtypeStruct((64, 64), BF16), j...]
    all_to_all x2 -> x0, waiting for transfers between devices: 31.8 us -> none  [from_everyone(): return lax.all_to_all(copies, axis, split_axis=0, concat_axis=0, tiled=True)]
    all_to_all x2 -> x0, starting transfers between devices: 19.7 us -> none  [from_everyone(): return lax.all_to_all(copies, axis, split_axis=0, concat_axis=0, tiled=True)]
    reshape x7 -> x0, local copies, waits for them, and re-layouts: 11.4 us -> none  [the longest x2 4.16 us: joined_along(): return jnp.moveaxis(tiles, 0, dim).reshape(dims)]
    dot_general x8 -> x0, matrix products: 10.6 us -> none  [the longest x5 4.4 us: project_flat(): jnp.dot(inputs, flattened, preferred_element_type=jnp.float32)]
    unnamed x31 -> x2, local copies, waits for them, and re-layouts: 14.5 us -> 4.42 us
    transpose x2 -> x0, local copies, waits for them, and re-layouts: 3.32 us -> none  [joined_along(): return jnp.moveaxis(tiles, 0, dim).reshape(dims)]
  transfers between devices with their start and end apart: 2 -> 0, of which waited for: 2 -> 0; matrix products, arithmetic and copies ran while one was open for 2% -> 0% of each run, Pallas kernels for 0% -> 0%
where the time goes in v1:
time: 73.4 us; the launch traced here: 73.2 us
  Pallas kernels  68.1 us (93%)
  local copies, waits for them, and re-layouts  4.42 us (6%)
    pallas_call x1, Pallas kernels, body(): pl.pallas_call(kernel, out_shape=(jax.ShapeDtypeStruct((64, 64), BF16), j...  68.1 us
    unnamed x2, local copies, waits for them, and re-layouts  4.42 us

profile of v1, /device:TPU:1, one launch (start us, length us, event | category | flops | bytes accessed | tf_op | source)
XLA Modules:
  0.0 73.2 jit_solution(4076089057819963419)
XLA Ops:
  0.6 68.1 %layer_step.1 = (bf16[64,64]{1,0:T(8,128)(2,1)}, f32[2,8,128,256]{3,2,1,0:T(8,128)}) custom-call(bf16[64,64]{1,0:T(8,128)(2,1)} %tok.1, bf16[8,4,4096]{2,1,0:T(4,128)(2,1)} %bitcast.17, bf16[8,4,4096]{2,1,0:T(4,128)(2,1)} %bitcast.18, bf16[8,4,4096]{2,1,0:T(4,128)(2,1)} %bitcast.19, bf16[64,4096]{1,0:T(8,128)(2,1)} %bitcast.14, bf16[64,4096]{1,0:T(8,128)(2,1)} %bitcast.15, ...), custom_call_target="tpu_custom_call" | custom-call | tf_op jit(solution)/shard_map/layer_step/pallas_call | solution.py:403
  68.8 1.3 %copy.20 = bf16[64,64]{1,0:T(8,128)(2,1)} copy(bf16[64,64]{1,0:T(8,128)(2,1)} %get-tuple-element.4) | data formatting | bytes 16384
  70.1 3.1 %copy.21 = f32[2,8,128,256]{3,2,1,0:T(8,128)} copy(f32[2,8,128,256]{3,2,1,0:T(8,128)} %get-tuple-element.5) | data formatting | bytes 4194304

commit v2 on v1

--- a/solution.py
+++ b/solution.py
@@ -20,6 +20,10 @@
 NN = (((1,), (0,)), ((), ()))
 TN = (((0,), (0,)), ((), ()))
 CHIPS = 32
+FAR = sorted(
+    ((d, e) for d in range(8) for e in range(4) if d or e),
+    key=lambda o: (-min(o[0], 8 - o[0]) - min(o[1], 4 - o[1]), o),
+)
 
 
 def dot(a, b, dims):
@@ -36,20 +40,21 @@
     wst, wc, owc, upc, dnc, st,
     s_a, r_a, s_g, r_g, x, s_b, r_b, ro, s_c, r_c, att32, att,
     s_e, r_e, s_m, r_m, xt, xn, s_y, r_y, s_h, r_h, s_f, r_f, sq,
-    own_sem, w_send, w_recv, st_out_sem,
-    a_sem, g_sem, b_sem, c_sem, e_sem, m_sem, y_sem, h_sem, f_sem,
+    own_sem, w_send, w_recv,
+    az_send, az_recv, ax_sem, g_sem, p_sem, b_sem, c_sem, e_sem, m_sem, y_sem, h_sem, f_sem,
 ):
     kv = lax.axis_index("kv")
     t = lax.axis_index("tp")
     z, xx = kv // 4, kv % 4
     half = kv // 16
     mine = half == t
-
-    def chip_at(j):
-        i = j // 4
-        dz = lax.rem(4 + ((i + 1) // 2) * (2 * lax.rem(i, 2) - 1) + 8, 8)
-        dx = lax.rem(j + 1, 4)
-        return lax.rem(z + dz, 8) * 4 + lax.rem(xx + dx, 4)
+    partner = 1 - t
+
+    def wrap(v, n):
+        return jnp.where(v >= n, v - n, v)
+
+    zd = [wrap(z + d, 8) for d in range(8)]
+    xd = [wrap(xx + d, 4) for d in range(4)]
 
     def rcopy(src, dst, sems, kv_to, t_to):
         return pltpu.make_async_remote_copy(
@@ -61,9 +66,9 @@
         pltpu.make_async_copy(ref, ref, sem).wait()
 
     own = [
-        pltpu.make_async_copy(wq, wst.at[t, 0], own_sem.at[0]),
-        pltpu.make_async_copy(wk, wst.at[t, 1], own_sem.at[1]),
-        pltpu.make_async_copy(wd, wst.at[t, 2], own_sem.at[2]),
+        pltpu.make_async_copy(wq, wst.at[0], own_sem.at[0]),
+        pltpu.make_async_copy(wk, wst.at[1], own_sem.at[1]),
+        pltpu.make_async_copy(wd, wst.at[2], own_sem.at[2]),
         pltpu.make_async_copy(wv, wc.at[t, pl.ds(96, 64)], own_sem.at[3]),
         pltpu.make_async_copy(wg, wc.at[t, pl.ds(160, 64)], own_sem.at[4]),
         pltpu.make_async_copy(states, st, own_sem.at[5]),
@@ -76,10 +81,15 @@
 
     barrier = pltpu.get_barrier_semaphore()
 
-    @pl.loop(1, 64)
-    def _(i):
-        p = lax.rem(kv * 2 + t + i, 64)
-        pl.semaphore_signal(barrier, inc=1, device_id={"kv": p // 2, "tp": lax.rem(p, 2)}, device_id_type=MESH)
+    def hello(kv_to, t_to):
+        pl.semaphore_signal(barrier, inc=1, device_id={"kv": kv_to, "tp": t_to}, device_id_type=MESH)
+
+    for d in (4, 3, 5, 2, 6, 1, 7):
+        hello(zd[d] * 4 + xx, t)
+        hello(zd[d] * 4 + xx, partner)
+    for d in (2, 1, 3):
+        hello(z * 4 + xd[d], t)
+    hello(kv, partner)
 
     tk = tok[...].astype(F32)
     for hh in range(2):
@@ -88,49 +98,9 @@
         ).astype(BF16)
     s_g[0:1] = jnp.concatenate([g1[...], b1[...]], axis=1)
     s_g[1:2] = jnp.concatenate([g2[...], b2[...]], axis=1)
-    me = t * CHIPS + kv
+    me = kv * 2 + t
     r_a[me] = s_a[t]
-    r_g[me] = s_g[...]
-    pl.semaphore_wait(barrier, 63)
-
-    @pl.loop(0, CHIPS)
-    def _(j):
-        kp = chip_at(j)
-        for tt in range(2):
-
-            @pl.when(jnp.logical_or(kp != kv, t != tt))
-            def _():
-                rcopy(s_a.at[tt], r_a.at[me], a_sem, kp, tt).start()
-
-    partner = 1 - t
-
-    def wcopy(src, dst, i):
-        return pltpu.make_async_remote_copy(
-            src_ref=src, dst_ref=dst, send_sem=w_send.at[i], recv_sem=w_recv.at[i],
-            device_id={"kv": kv, "tp": partner}, device_id_type=MESH,
-        )
-
-    wcopies = [
-        wcopy(wq, wst.at[t, 0], 0),
-        wcopy(wk, wst.at[t, 1], 1),
-        wcopy(wd, wst.at[t, 2], 2),
-        wcopy(wv, wc.at[t, pl.ds(96, 64)], 3),
-        wcopy(wg, wc.at[t, pl.ds(160, 64)], 4),
-        wcopy(ow, owc.at[t], 5),
-        wcopy(up, upc.at[t], 6),
-        wcopy(dn, dnc.at[t], 7),
-    ]
-    for c in wcopies[:5]:
-        c.start()
-
-    @pl.loop(0, CHIPS)
-    def _(j):
-        kp = chip_at(j)
-        for tt in range(2):
-
-            @pl.when(jnp.logical_or(kp != kv, t != tt))
-            def _():
-                rcopy(s_g, r_g.at[me], g_sem, kp, tt).start()
+    r_g[t, kv] = s_g[...]
 
     lane = iota((16, 128), 1) < 64
     col = iota((224, 256), 1)
@@ -148,41 +118,78 @@
         [zero(16), bias[...], zero(24), bias[...], zero(8 + 64)], axis=0
     ).T[:, :64]
 
-    for c in own:
+    for c in own[:5]:
         c.wait()
-    for c in wcopies[:5]:
-        c.wait()
-    for c in wcopies[5:]:
-        c.start()
-    for tt in range(2):
-        for ty in range(3):
-            for h in range(0, 8, 4):
-                wc[tt, ty * 32 + h * 4 : ty * 32 + h * 4 + 16, :] = jnp.concatenate(
-                    [wst[tt, ty, h + i].astype(F32) for i in range(4)], axis=0
-                ).astype(BF16)
-
-    drain(r_a.at[pl.ds(0, 63)], a_sem.at[1])
+    for ty in range(3):
+        for h in range(0, 8, 4):
+            wc[t, ty * 32 + h * 4 : ty * 32 + h * 4 + 16, :] = jnp.concatenate(
+                [wst[ty, h + i].astype(F32) for i in range(4)], axis=0
+            ).astype(BF16)
+
+    def wcopy(ref, i):
+        return pltpu.make_async_remote_copy(
+            src_ref=ref.at[t], dst_ref=ref.at[t], send_sem=w_send.at[i], recv_sem=w_recv.at[i],
+            device_id={"kv": kv, "tp": partner}, device_id_type=MESH,
+        )
+
+    wcopies = [wcopy(wc, 0), wcopy(owc, 1), wcopy(upc, 2), wcopy(dnc, 3)]
+    pl.semaphore_wait(barrier, 18)
+
+    def to_line(src, kv_to, t_to):
+        pltpu.make_async_remote_copy(
+            src_ref=src, dst_ref=r_a.at[me], send_sem=az_send, recv_sem=az_recv.at[z * 2 + t],
+            device_id={"kv": kv_to, "tp": t_to}, device_id_type=MESH,
+        ).start()
+
+    to_line(s_a.at[partner], kv, partner)
+    for d in (4, 3, 5, 2, 6, 1, 7):
+        for tt in range(2):
+            to_line(s_a.at[tt], zd[d] * 4 + xx, tt)
+    wcopies[0].start()
+    for d in (0, 1, 7, 2, 6, 3, 5, 4):
+        if d == 0:
+            drain(r_a.at[0], az_recv.at[z * 2 + partner])
+        else:
+            drain(r_a.at[0], az_recv.at[zd[d] * 2])
+            drain(r_a.at[0], az_recv.at[zd[d] * 2 + 1])
+        block = r_a.at[pl.ds((zd[d] * 4 + xx) * 2, 2)]
+        for e in (2, 1, 3):
+            rcopy(block, block, ax_sem, z * 4 + xd[e], t).start()
+    drain(r_a.at[pl.ds(0, 48)], ax_sem.at[1])
     for c in range(CHIPS):
-        a0 = r_a[c].astype(F32)
-        a1 = r_a[CHIPS + c].astype(F32)
+        a0 = r_a[2 * c].astype(F32)
+        a1 = r_a[2 * c + 1].astype(F32)
         x[0:16, c * 128 : (c + 1) * 128] = jnp.where(lane, a0, pltpu.roll(a1, 64, 1)).astype(BF16)
         x[16:32, c * 128 : (c + 1) * 128] = jnp.where(lane, pltpu.roll(a0, 64, 1), a1).astype(BF16)
 
+    wcopies[0].wait()
     for tt in range(2):
         p = dot(x[...], wc[tt], NT).astype(BF16)
         p = dot(p, perm, NN)
         for i in range(16):
             s_b[i, tt] = p[2 * i : 2 * i + 2, :]
 
-    @pl.loop(0, 16)
-    def _(i):
-        k16 = lax.rem(kv + 8 + i, 16)
-        kp = 16 * t + k16
-        for tt in range(2):
-
-            @pl.when(jnp.logical_or(kp != kv, t != tt))
-            def _():
-                rcopy(s_b.at[k16, tt], r_b.at[kv], b_sem, kp, tt).start()
+    for i in range(4):
+        zl = wrap(z - 4 * half + i, 4)
+        for j in (2, 1, 3, 0):
+            k16 = zl * 4 + xd[j]
+            kp = 16 * t + k16
+            for tt in range(2):
+                if i == 0 and j == 0:
+
+                    @pl.when(jnp.logical_not(jnp.logical_and(mine, t == tt)))
+                    def _():
+                        rcopy(s_b.at[k16, tt], r_b.at[kv], b_sem, kp, tt).start()
+
+                else:
+                    rcopy(s_b.at[k16, tt], r_b.at[kv], b_sem, kp, tt).start()
+
+    for i in range(1, 4):
+        own[5 + i].wait()
+        wcopies[i].start()
+    for d, e in FAR:
+        rcopy(s_g, r_g.at[t, kv], g_sem, zd[d] * 4 + xd[e], t).start()
+    own[5].wait()
 
     @pl.when(mine)
     def _():
@@ -208,10 +215,8 @@
         for h in range(8):
             o = s * 32 + h
             new = retain[:, o + 16 : o + 17] * st[s, h] + cols[:, o + 8 : o + 9] * rows[s][h : h + 1, :]
-            st[s, h] = new
+            new_states[s, h] = new
             ro[s * 8 + h : s * 8 + h + 1, :] = jnp.sum(q[:, o : o + 1] * new, axis=0, keepdims=True)
-    st_out = pltpu.make_async_copy(st, new_states, st_out_sem)
-    st_out.start()
     readout = ro[...]
     gate = jnp.concatenate([rows[0][8:16], rows[1][8:16]], axis=0)
     hg = jnp.concatenate([head_gain[...], head_gain[...]], axis=0)
@@ -220,13 +225,16 @@
 
     slot_c = t * 16 + lax.rem(kv, 16)
 
-    @pl.loop(0, CHIPS)
-    def _(j):
-        kp = chip_at(j)
-
-        @pl.when(jnp.logical_or(kp != kv, t != half))
-        def _():
-            rcopy(s_c, r_c.at[slot_c], c_sem, kp, half).start()
+    for d, e in FAR:
+        rcopy(s_c, r_c.at[slot_c], c_sem, zd[d] * 4 + xd[e], half).start()
+
+    @pl.when(jnp.logical_not(mine))
+    def _():
+        rcopy(s_c, r_c.at[slot_c], c_sem, kv, half).start()
+
+    drain(r_g.at[t, pl.ds(0, 31)], g_sem.at[1])
+    gains = rcopy(r_g.at[t], r_g.at[t], p_sem, kv, partner)
+    gains.start()
 
     @pl.when(mine)
     def _():
@@ -244,7 +252,7 @@
             for h in range(8):
                 at = tt * 2048 + h * 256 + n * 128
                 att[:, at : at + 128] = att32[n, pl.ds(h, 32, stride=8), :].astype(BF16)
-    wcopies[5].wait()
+    wcopies[1].wait()
     mixed = jnp.concatenate([dot(att[...], owc[tt], NT) for tt in range(2)], axis=1)
     at_chip = pl.multiple_of(kv * 128, 128)
     res1 = ALPHA * x[:, pl.ds(at_chip, 128)].astype(F32) + mixed
@@ -255,22 +263,21 @@
     s_m[...] = sq[...].T[0:1, :]
     s_e[...] = (res1 - m_own).astype(BF16)
 
-    @pl.loop(0, CHIPS - 1)
-    def _(j):
-        kp = chip_at(j)
+    for d, e in FAR:
+        kp = zd[d] * 4 + xd[e]
         rcopy(s_e, r_e.at[kv], e_sem, kp, t).start()
         rcopy(s_m, r_m.at[kv], m_sem, kp, t).start()
 
     r_e[kv] = s_e[...]
     r_m[kv] = s_m[...]
-    drain(r_g.at[pl.ds(0, 63)], g_sem.at[1])
-    ga = r_g[0:32, 0, :]
-    gb = r_g[32:64, 0, :]
+    gains.wait()
+    ga = r_g[0, :, 0, :]
+    gb = r_g[1, :, 0, :]
     lane32 = iota((32, 128), 1) < 64
     gain1 = jnp.where(lane32, ga, pltpu.roll(gb, 64, 1))
     bias1 = jnp.where(lane32, pltpu.roll(ga, 64, 1), gb)
-    wcopies[6].wait()
-    wcopies[7].wait()
+    wcopies[2].wait()
+    wcopies[3].wait()
     drain(r_m.at[pl.ds(0, 31)], m_sem.at[1])
     drain(r_e.at[pl.ds(0, 31)], e_sem.at[1])
     sq[0:32, :] = r_m[:, 0, :]
@@ -292,17 +299,15 @@
     for tt in range(2):
         lifted = jnp.maximum(dot(xn[...], upc[tt], NN), 0.0)
         hidden.append((lifted * lifted).astype(BF16))
-
-    @pl.loop(0, CHIPS)
-    def _(j):
-        kp = chip_at(j)
-        cl = pl.ds(pl.multiple_of(kp * 128, 128), 128)
-        y = dot(hidden[0], dnc[0, :, cl], NN) + dot(hidden[1], dnc[1, :, cl], NN)
-        s_y[kp] = y.astype(BF16)
-
-        @pl.when(kp != kv)
-        def _():
-            rcopy(s_y.at[kp], r_y.at[kv], y_sem, kp, t).start()
+    for d in (4, 3, 5, 2, 6, 1, 7, 0):
+        cl = pl.ds(pl.multiple_of(zd[d] * 512, 512), 512)
+        y = (dot(hidden[0], dnc[0, :, cl], NN) + dot(hidden[1], dnc[1, :, cl], NN)).astype(BF16)
+        for j in range(4):
+            s_y[zd[d] * 4 + j] = y[:, j * 128 : (j + 1) * 128]
+        for e in (2, 1, 3, 0):
+            if d or e:
+                kp = zd[d] * 4 + xd[e]
+                rcopy(s_y.at[kp], r_y.at[kv], y_sem, kp, t).start()
 
     r_y[kv] = s_y[kv]
     drain(r_y.at[pl.ds(0, 31)], y_sem.at[1])
@@ -316,9 +321,8 @@
     sq[0:32, :] = jnp.where(iota((32, 128), 1) == 0, m_own, v_own)
     s_h[...] = sq[...].T[0:2, :]
 
-    @pl.loop(0, CHIPS - 1)
-    def _(j):
-        rcopy(s_h, r_h.at[kv], h_sem, chip_at(j), t).start()
+    for d, e in FAR:
+        rcopy(s_h, r_h.at[kv], h_sem, zd[d] * 4 + xd[e], t).start()
 
     r_h[kv] = s_h[...]
     drain(r_h.at[pl.ds(0, 31)], h_sem.at[1])
@@ -331,8 +335,8 @@
     sq[0:1, :] = mean
     sq[1:2, :] = inv
     back = sq[...].T
-    own0 = r_g[kv][1:2, :]
-    own1 = r_g[CHIPS + kv][1:2, :]
+    own0 = r_g[0, kv][1:2, :]
+    own1 = r_g[1, kv][1:2, :]
     lane1 = iota((1, 128), 1) < 64
     gain2 = jnp.where(lane1, own0, pltpu.roll(own1, 64, 1))
     bias2 = jnp.where(lane1, pltpu.roll(own0, 64, 1), own1)
@@ -346,8 +350,9 @@
     f = r_f[...].astype(F32)
     out[pl.ds(pl.multiple_of(partner * 32, 32), 32), :] = jnp.where(first, f, pltpu.roll(f, 64, 1))[:, :64].astype(BF16)
 
-    drain(r_a.at[pl.ds(0, 63)], a_sem.at[0])
-    drain(r_g.at[pl.ds(0, 63)], g_sem.at[0])
+    drain(r_a.at[pl.ds(0, 15)], az_send)
+    drain(r_a.at[pl.ds(0, 48)], ax_sem.at[0])
+    drain(r_g.at[t, pl.ds(0, 31)], g_sem.at[0])
 
     @pl.when(mine)
     def _():
@@ -363,7 +368,6 @@
     drain(r_m.at[pl.ds(0, 31)], m_sem.at[0])
     drain(r_y.at[pl.ds(0, 31)], y_sem.at[0])
     drain(r_h.at[pl.ds(0, 31)], h_sem.at[0])
-    st_out.wait()
 
 
 def body(
@@ -378,14 +382,14 @@
     V = pltpu.VMEM
     dma = pltpu.SemaphoreType.DMA
     scratch = [
-        V((2, 3, 8, 4, D), BF16),
+        V((3, 8, 4, D), BF16),
         V((2, 224, D), BF16),
         V((2, 64, D), BF16),
         V((2, D, 256), BF16),
         V((2, 256, D), BF16),
         V((2, 8, 128, 256), F32),
         V((2, 16, 128), BF16), V((64, 16, 128), BF16),
-        V((2, 128), F32), V((64, 2, 128), F32),
+        V((2, 128), F32), V((2, 32, 2, 128), F32),
         V((32, D), BF16),
         V((16, 2, 2, 256), F32), V((32, 2, 256), F32),
         V((16, 256), F32),
@@ -398,16 +402,16 @@
         V((2, 128), F32), V((32, 2, 128), F32),
         V((32, 128), BF16), V((32, 128), BF16),
         V((128, 128), F32),
-        dma((9,)), dma((8,)), dma((8,)), dma,
-    ] + [dma((2,))] * 9
+        dma((9,)), dma((4,)), dma((4,)), dma, dma((16,)),
+    ] + [dma((2,))] * 10
     return pl.pallas_call(
         kernel,
         out_shape=(
-            jax.ShapeDtypeStruct((64, 64), BF16),
-            jax.ShapeDtypeStruct((2, 8, 128, 256), F32),
+            pltpu.VMEM((64, 64), BF16),
+            pltpu.VMEM((2, 8, 128, 256), F32),
         ),
         in_specs=[vmem] + [hbm] * 5 + [vmem, hbm, vmem, hbm, vmem, vmem, hbm, hbm, vmem, vmem],
-        out_specs=(vmem, hbm),
+        out_specs=(vmem, vmem),
         scratch_shapes=scratch,
         compiler_params=pltpu.CompilerParams(
             collective_id=0, has_side_effects=True, vmem_limit_bytes=60 * 1024 * 1024

time: 73.4 us -> 65.2 us (0.89)
  Pallas kernels: 68.1 us -> 62.5 us
  local copies, waits for them, and re-layouts: 4.42 us -> 1.93 us
    pallas_call x1, Pallas kernels: 68.1 us -> 62.5 us  [body(): pl.pallas_call(kernel, out_shape=(pltpu.VMEM((64, 64), BF16), pltpu.VMEM(...]
    unnamed x2, local copies, waits for them, and re-layouts: 4.42 us -> 1.93 us
where the time goes in v2:
time: 65.2 us; the launch traced here: 65.1 us
  Pallas kernels  62.5 us (96%)
  local copies, waits for them, and re-layouts  1.93 us (3%)
    pallas_call x1, Pallas kernels, body(): pl.pallas_call(kernel, out_shape=(pltpu.VMEM((64, 64), BF16), pltpu.VMEM(...  62.5 us
    unnamed x2, local copies, waits for them, and re-layouts  1.93 us

profile of v2, /device:TPU:1, one launch (start us, length us, event | category | flops | bytes accessed | tf_op | source)
XLA Modules:
  0.0 65.1 jit_solution(10135263486622458505)
XLA Ops:
  0.6 62.5 %layer_step.1 = (bf16[64,64]{1,0:T(8,128)(2,1)S(1)}, f32[2,8,128,256]{3,2,1,0:T(8,128)S(1)}) custom-call(bf16[64,64]{1,0:T(8,128)(2,1)} %tok.1, bf16[8,4,4096]{2,1,0:T(4,128)(2,1)} %bitcast.17, bf16[8,4,4096]{2,1,0:T(4,128)(2,1)} %bitcast.18, bf16[8,4,4096]{2,1,0:T(4,128)(2,1)} %bitcast.19, bf16[64,4096]{1,0:T(8,128)(2,1)} %bitcast.14, ...), custom_call_target="tpu_custom_call" | custom-call | tf_op jit(solution)/shard_map/layer_step/pallas_call | solution.py:407
  63.1 0.6 copy.20
  63.8 1.3 %copy.21 = f32[2,8,128,256]{3,2,1,0:T(8,128)} copy(f32[2,8,128,256]{3,2,1,0:T(8,128)S(1)} %get-tuple-element.3) | data formatting | bytes 4194304

commit v3 on v2

--- a/solution.py
+++ b/solution.py
@@ -24,6 +24,7 @@
     ((d, e) for d in range(8) for e in range(4) if d or e),
     key=lambda o: (-min(o[0], 8 - o[0]) - min(o[1], 4 - o[1]), o),
 )
+NEAR = (1, 7, 2, 6)
 
 
 def dot(a, b, dims):
@@ -35,13 +36,13 @@
 
 
 def kernel(
-    tok, wq, wk, wd, wv, wg, bias, states, head_gain, ow, g1, b1, up, dn, g2, b2,
+    tok_h, wq, wk, wd, wv, wg, bias_h, states, head_gain_h, ow, g1_h, b1_h, up, dn, g2_h, b2_h,
     out, new_states,
-    wst, wc, owc, upc, dnc, st,
+    tok, bias, head_gain, g1, b1, g2, b2, wst, wc, owc, upc, dnc, st,
     s_a, r_a, s_g, r_g, x, s_b, r_b, ro, s_c, r_c, att32, att,
     s_e, r_e, s_m, r_m, xt, xn, s_y, r_y, s_h, r_h, s_f, r_f, sq,
-    own_sem, w_send, w_recv,
-    az_send, az_recv, ax_sem, g_sem, p_sem, b_sem, c_sem, e_sem, m_sem, y_sem, h_sem, f_sem,
+    small_sem, own_sem, w_send, w_recv,
+    az_send, az_recv, ax_send, ax_recv, g_sem, p_sem, b_sem, c_send, c_recv, e_send, e_recv, m_sem, y_sem, h_sem, f_sem,
 ):
     kv = lax.axis_index("kv")
     t = lax.axis_index("tp")
@@ -64,6 +65,27 @@
 
     def drain(ref, sem):
         pltpu.make_async_copy(ref, ref, sem).wait()
+
+    barrier = pltpu.get_barrier_semaphore()
+
+    def hello(kv_to, t_to):
+        pl.semaphore_signal(barrier, inc=1, device_id={"kv": kv_to, "tp": t_to}, device_id_type=MESH)
+
+    for d in (4, 3, 5, 2, 6, 1, 7):
+        hello(zd[d] * 4 + xx, t)
+        hello(zd[d] * 4 + xx, partner)
+    for d in (2, 1, 3):
+        hello(z * 4 + xd[d], t)
+    hello(kv, partner)
+
+    small = [
+        pltpu.make_async_copy(a, b, small_sem.at[i])
+        for i, (a, b) in enumerate(
+            [(tok_h, tok), (bias_h, bias), (head_gain_h, head_gain), (g1_h, g1), (b1_h, b1), (g2_h, g2), (b2_h, b2)]
+        )
+    ]
+    for c in small:
+        c.start()
 
     own = [
         pltpu.make_async_copy(wq, wst.at[0], own_sem.at[0]),
@@ -79,18 +101,8 @@
     for c in own:
         c.start()
 
-    barrier = pltpu.get_barrier_semaphore()
-
-    def hello(kv_to, t_to):
-        pl.semaphore_signal(barrier, inc=1, device_id={"kv": kv_to, "tp": t_to}, device_id_type=MESH)
-
-    for d in (4, 3, 5, 2, 6, 1, 7):
-        hello(zd[d] * 4 + xx, t)
-        hello(zd[d] * 4 + xx, partner)
-    for d in (2, 1, 3):
-        hello(z * 4 + xd[d], t)
-    hello(kv, partner)
-
+    for c in small:
+        c.wait()
     tk = tok[...].astype(F32)
     for hh in range(2):
         s_a[hh] = jnp.concatenate(
@@ -154,17 +166,29 @@
             drain(r_a.at[0], az_recv.at[zd[d] * 2 + 1])
         block = r_a.at[pl.ds((zd[d] * 4 + xx) * 2, 2)]
         for e in (2, 1, 3):
-            rcopy(block, block, ax_sem, z * 4 + xd[e], t).start()
-    drain(r_a.at[pl.ds(0, 48)], ax_sem.at[1])
-    for c in range(CHIPS):
-        a0 = r_a[2 * c].astype(F32)
-        a1 = r_a[2 * c + 1].astype(F32)
-        x[0:16, c * 128 : (c + 1) * 128] = jnp.where(lane, a0, pltpu.roll(a1, 64, 1)).astype(BF16)
-        x[16:32, c * 128 : (c + 1) * 128] = jnp.where(lane, pltpu.roll(a0, 64, 1), a1).astype(BF16)
+            pltpu.make_async_remote_copy(
+                src_ref=block, dst_ref=block, send_sem=ax_send, recv_sem=ax_recv.at[zd[d]],
+                device_id={"kv": z * 4 + xd[e], "tp": t}, device_id_type=MESH,
+            ).start()
 
     wcopies[0].wait()
+    projected = [jnp.zeros((32, 224), F32) for _ in range(2)]
+    for d in (0, 1, 7, 2, 6, 3, 5, 4):
+        drain(r_a.at[pl.ds(0, 6)], ax_recv.at[zd[d]])
+        tiles = []
+        for j in range(4):
+            a0 = r_a[zd[d] * 8 + 2 * j].astype(F32)
+            a1 = r_a[zd[d] * 8 + 2 * j + 1].astype(F32)
+            low = jnp.where(lane, a0, pltpu.roll(a1, 64, 1))
+            high = jnp.where(lane, pltpu.roll(a0, 64, 1), a1)
+            tiles.append(jnp.concatenate([low, high], axis=0).astype(BF16))
+        tile = jnp.concatenate(tiles, axis=1)
+        cl = pl.ds(pl.multiple_of(zd[d] * 512, 512), 512)
+        x[:, cl] = tile
+        for tt in range(2):
+            projected[tt] = projected[tt] + dot(tile, wc[tt, :, cl], NT)
     for tt in range(2):
-        p = dot(x[...], wc[tt], NT).astype(BF16)
+        p = projected[tt].astype(BF16)
         p = dot(p, perm, NN)
         for i in range(16):
             s_b[i, tt] = p[2 * i : 2 * i + 2, :]
@@ -225,25 +249,54 @@
 
     slot_c = t * 16 + lax.rem(kv, 16)
 
+    def send_c(src, slot, kv_to, t_to):
+        pltpu.make_async_remote_copy(
+            src_ref=src, dst_ref=r_c.at[slot], send_sem=c_send, recv_sem=c_recv.at[slot],
+            device_id={"kv": kv_to, "tp": t_to}, device_id_type=MESH,
+        ).start()
+
     for d, e in FAR:
-        rcopy(s_c, r_c.at[slot_c], c_sem, zd[d] * 4 + xd[e], half).start()
+        if e == 0 or d not in NEAR:
+            send_c(s_c, slot_c, zd[d] * 4 + xd[e], half)
 
     @pl.when(jnp.logical_not(mine))
     def _():
-        rcopy(s_c, r_c.at[slot_c], c_sem, kv, half).start()
+        send_c(s_c, slot_c, kv, half)
+
+    @pl.when(mine)
+    def _():
+        r_c[slot_c] = s_c[...]
+
+    for d in NEAR:
+
+        @pl.when(zd[d] // 4 == t)
+        def _():
+            for tt in range(2):
+                slot = tt * 16 + (zd[d] - 4 * t) * 4 + xx
+                drain(s_c, c_recv.at[slot])
+                for e in (2, 1, 3):
+                    send_c(r_c.at[slot], slot, z * 4 + xd[e], t)
 
     drain(r_g.at[t, pl.ds(0, 31)], g_sem.at[1])
     gains = rcopy(r_g.at[t], r_g.at[t], p_sem, kv, partner)
     gains.start()
 
-    @pl.when(mine)
-    def _():
-        r_c[slot_c] = s_c[...]
-        drain(r_c.at[pl.ds(0, 31)], c_sem.at[1])
-
-    @pl.when(jnp.logical_not(mine))
-    def _():
-        drain(r_c, c_sem.at[1])
+    for d in range(8):
+        for e in range(4):
+            if e == 0 and d in NEAR:
+                continue
+
+            @pl.when(zd[d] // 4 == t)
+            def _():
+                for tt in range(2):
+                    slot = tt * 16 + (zd[d] - 4 * t) * 4 + xd[e]
+                    if d or e:
+                        drain(s_c, c_recv.at[slot])
+                    else:
+
+                        @pl.when(t != tt)
+                        def _():
+                            drain(s_c, c_recv.at[slot])
 
     for tt in range(2):
         arrived = r_c[tt * 16 : (tt + 1) * 16].astype(F32).reshape(256, 256)
@@ -263,11 +316,22 @@
     s_m[...] = sq[...].T[0:1, :]
     s_e[...] = (res1 - m_own).astype(BF16)
 
+    def send_e(src, slot, kv_to):
+        pltpu.make_async_remote_copy(
+            src_ref=src, dst_ref=r_e.at[slot], send_sem=e_send, recv_sem=e_recv.at[slot],
+            device_id={"kv": kv_to, "tp": t}, device_id_type=MESH,
+        ).start()
+
     for d, e in FAR:
-        kp = zd[d] * 4 + xd[e]
-        rcopy(s_e, r_e.at[kv], e_sem, kp, t).start()
-        rcopy(s_m, r_m.at[kv], m_sem, kp, t).start()
-
+        if e == 0 or d not in NEAR:
+            send_e(s_e, kv, zd[d] * 4 + xd[e])
+    for d, e in FAR:
+        rcopy(s_m, r_m.at[kv], m_sem, zd[d] * 4 + xd[e], t).start()
+    for d in NEAR:
+        slot = zd[d] * 4 + xx
+        drain(s_e, e_recv.at[slot])
+        for e in (2, 1, 3):
+            send_e(r_e.at[slot], slot, z * 4 + xd[e])
     r_e[kv] = s_e[...]
     r_m[kv] = s_m[...]
     gains.wait()
@@ -279,7 +343,9 @@
     wcopies[2].wait()
     wcopies[3].wait()
     drain(r_m.at[pl.ds(0, 31)], m_sem.at[1])
-    drain(r_e.at[pl.ds(0, 31)], e_sem.at[1])
+    for d, e in FAR:
+        if e or d not in NEAR:
+            drain(s_e, e_recv.at[zd[d] * 4 + xd[e]])
     sq[0:32, :] = r_m[:, 0, :]
     means = sq[...].T[0:32, 0:32]
     acc = jnp.zeros((32, 128), F32)
@@ -319,55 +385,62 @@
     dev = res2 - m_own
     v_own = jnp.sum(dev * dev, axis=-1, keepdims=True)
     sq[0:32, :] = jnp.where(iota((32, 128), 1) == 0, m_own, v_own)
-    s_h[...] = sq[...].T[0:2, :]
-
+    flat = sq[...].T
+    s_h[...] = jnp.concatenate([flat[0:1, 0:32], flat[1:2, 0:32], flat[0:1, 0:64]], axis=1)
+    s_f[...] = res2
+    last = rcopy(s_f, r_f, f_sem, kv, partner)
     for d, e in FAR:
-        rcopy(s_h, r_h.at[kv], h_sem, zd[d] * 4 + xd[e], t).start()
-
-    r_h[kv] = s_h[...]
-    drain(r_h.at[pl.ds(0, 31)], h_sem.at[1])
-    ms = r_h[:, 0, :]
-    vs = r_h[:, 1, :]
-    mean = jnp.mean(ms, axis=0, keepdims=True)
-    dm = ms - mean
-    spread = (jnp.sum(vs, axis=0, keepdims=True) + 128.0 * jnp.sum(dm * dm, axis=0, keepdims=True)) / D
-    inv = lax.rsqrt(spread + LN_EPS)
-    sq[0:1, :] = mean
-    sq[1:2, :] = inv
-    back = sq[...].T
+        for tt in range(2):
+            rcopy(s_h, r_h.at[t * CHIPS + kv], h_sem, zd[d] * 4 + xd[e], tt).start()
+    rcopy(s_h, r_h.at[t * CHIPS + kv], h_sem, kv, partner).start()
+    last.start()
+    r_h[t * CHIPS + kv] = s_h[...]
     own0 = r_g[0, kv][1:2, :]
     own1 = r_g[1, kv][1:2, :]
     lane1 = iota((1, 128), 1) < 64
     gain2 = jnp.where(lane1, own0, pltpu.roll(own1, 64, 1))
     bias2 = jnp.where(lane1, pltpu.roll(own0, 64, 1), own1)
-    o = ((res2 - back[0:32, 0:1]) * back[0:32, 1:2] * gain2 + bias2)
-    s_f[...] = o.astype(BF16)
-    last = rcopy(s_f, r_f, f_sem, kv, partner)
-    last.start()
-    first = t == 0
-    out[pl.ds(pl.multiple_of(t * 32, 32), 32), :] = jnp.where(first, o, pltpu.roll(o, 64, 1))[:, :64].astype(BF16)
     last.wait()
-    f = r_f[...].astype(F32)
-    out[pl.ds(pl.multiple_of(partner * 32, 32), 32), :] = jnp.where(first, f, pltpu.roll(f, 64, 1))[:, :64].astype(BF16)
+    drain(r_h.at[pl.ds(0, 63)], h_sem.at[1])
+    for tt in range(2):
+        ms = r_h[tt * CHIPS : (tt + 1) * CHIPS, 0, :]
+        mean = jnp.mean(ms, axis=0, keepdims=True)
+        dm = ms - mean
+        first = jnp.sum(ms, axis=0, keepdims=True)
+        spread = (first + pltpu.roll(128.0 * jnp.sum(dm * dm, axis=0, keepdims=True), 32, 1)) / D
+        sq[2 * tt : 2 * tt + 1, :] = mean
+        sq[2 * tt + 1 : 2 * tt + 2, :] = lax.rsqrt(spread + LN_EPS)
+    back = sq[...].T
+    for tt in range(2):
+        rows2 = jnp.where(t == tt, res2, r_f[...])
+        o = (rows2 - back[0:32, 2 * tt : 2 * tt + 1]) * back[32:64, 2 * tt + 1 : 2 * tt + 2] * gain2 + bias2
+        out[32 * tt : 32 * tt + 32, :] = jnp.where(t == 0, o, pltpu.roll(o, 64, 1))[:, :64].astype(BF16)
 
     drain(r_a.at[pl.ds(0, 15)], az_send)
-    drain(r_a.at[pl.ds(0, 48)], ax_sem.at[0])
+    drain(r_a.at[pl.ds(0, 48)], ax_send)
     drain(r_g.at[t, pl.ds(0, 31)], g_sem.at[0])
+    sent = 3 + sum(1 if d in NEAR else 4 for d in range(1, 8))
+    drain(r_c.at[pl.ds(0, sent)], c_send)
 
     @pl.when(mine)
     def _():
         drain(r_b.at[pl.ds(0, 31)], b_sem.at[0])
-        drain(r_c.at[pl.ds(0, 31)], c_sem.at[0])
 
     @pl.when(jnp.logical_not(mine))
     def _():
         drain(r_b, b_sem.at[0])
-        drain(r_c, c_sem.at[0])
-
-    drain(r_e.at[pl.ds(0, 31)], e_sem.at[0])
+        drain(s_c, c_send)
+
+    for d in NEAR:
+
+        @pl.when(zd[d] // 4 == t)
+        def _():
+            drain(r_c.at[pl.ds(0, 6)], c_send)
+
+    drain(r_e.at[pl.ds(0, 31)], e_send)
     drain(r_m.at[pl.ds(0, 31)], m_sem.at[0])
     drain(r_y.at[pl.ds(0, 31)], y_sem.at[0])
-    drain(r_h.at[pl.ds(0, 31)], h_sem.at[0])
+    drain(r_h.at[pl.ds(0, 63)], h_sem.at[0])
 
 
 def body(
@@ -382,6 +455,8 @@
     V = pltpu.VMEM
     dma = pltpu.SemaphoreType.DMA
     scratch = [
+        V((64, 64), BF16), V((8, 128), F32), V((8, 256), F32),
+        V((1, 64), F32), V((1, 64), F32), V((1, 64), F32), V((1, 64), F32),
         V((3, 8, 4, D), BF16),
         V((2, 224, D), BF16),
         V((2, 64, D), BF16),
@@ -399,18 +474,19 @@
         V((1, 128), F32), V((32, 1, 128), F32),
         V((32, 32, 128), F32), V((32, D), BF16),
         V((32, 32, 128), BF16), V((32, 32, 128), BF16),
-        V((2, 128), F32), V((32, 2, 128), F32),
-        V((32, 128), BF16), V((32, 128), BF16),
+        V((1, 128), F32), V((64, 1, 128), F32),
+        V((32, 128), F32), V((32, 128), F32),
         V((128, 128), F32),
-        dma((9,)), dma((4,)), dma((4,)), dma, dma((16,)),
-    ] + [dma((2,))] * 10
+        dma((7,)), dma((9,)), dma((4,)), dma((4,)), dma, dma((16,)), dma, dma((8,)),
+        dma((2,)), dma((2,)), dma((2,)), dma, dma((32,)), dma, dma((32,)),
+    ] + [dma((2,))] * 4
     return pl.pallas_call(
         kernel,
         out_shape=(
             pltpu.VMEM((64, 64), BF16),
             pltpu.VMEM((2, 8, 128, 256), F32),
         ),
-        in_specs=[vmem] + [hbm] * 5 + [vmem, hbm, vmem, hbm, vmem, vmem, hbm, hbm, vmem, vmem],
+        in_specs=[hbm] * 16,
         out_specs=(vmem, vmem),
         scratch_shapes=scratch,
         compiler_params=pltpu.CompilerParams(

time: 65.2 us -> 65.2 us (level)
  no operation moved by 1% of the time
where the time goes in v3:
time: 65.2 us; the launch traced here: 65.1 us
  Pallas kernels  62.5 us (96%)
  local copies, waits for them, and re-layouts  1.93 us (3%)
    pallas_call x1, Pallas kernels, body(): pl.pallas_call(kernel, out_shape=(pltpu.VMEM((64, 64), BF16), pltpu.VMEM(...  62.5 us
    unnamed x2, local copies, waits for them, and re-layouts  1.93 us

profile of v3, /device:TPU:1, one launch (start us, length us, event | category | flops | bytes accessed | tf_op | source)
XLA Modules:
  0.0 65.1 jit_solution(6898183182982680493)
XLA Ops:
  0.6 62.5 %layer_step.1 = (bf16[64,64]{1,0:T(8,128)(2,1)S(1)}, f32[2,8,128,256]{3,2,1,0:T(8,128)S(1)}) custom-call(bf16[64,64]{1,0:T(8,128)(2,1)} %tok_h.1, bf16[8,4,4096]{2,1,0:T(4,128)(2,1)} %bitcast.17, bf16[8,4,4096]{2,1,0:T(4,128)(2,1)} %bitcast.18, bf16[8,4,4096]{2,1,0:T(4,128)(2,1)} %bitcast.19, bf16[64,4096]{1,0:T(8,128)(2,1)} %bitcast.14, ...), custom_call_target="tpu_custom_call" | custom-call | tf_op jit(solution)/shard_map/layer_step/pallas_call | solution.py:483
  63.1 0.6 copy.20
  63.8 1.3 %copy.21 = f32[2,8,128,256]{3,2,1,0:T(8,128)} copy(f32[2,8,128,256]{3,2,1,0:T(8,128)S(1)} %get-tuple-element.3) | data formatting | bytes 4194304

commit v4 on v3

--- a/solution.py
+++ b/solution.py
@@ -24,7 +24,7 @@
     ((d, e) for d in range(8) for e in range(4) if d or e),
     key=lambda o: (-min(o[0], 8 - o[0]) - min(o[1], 4 - o[1]), o),
 )
-NEAR = (1, 7, 2, 6)
+NEAR = (1, 7, 2, 6, 3, 5, 4)
 
 
 def dot(a, b, dims):

time: 65.2 us -> 62.7 us (0.962)
  Pallas kernels: 62.5 us -> 60 us
    pallas_call x1, Pallas kernels: 62.5 us -> 60 us  [body(): pl.pallas_call(kernel, out_shape=(pltpu.VMEM((64, 64), BF16), pltpu.VMEM(...]
where the time goes in v4:
time: 62.7 us; the launch traced here: 62.6 us
  Pallas kernels  60 us (96%)
  local copies, waits for them, and re-layouts  1.93 us (3%)
  between operations  0.65 us (1%)
    pallas_call x1, Pallas kernels, body(): pl.pallas_call(kernel, out_shape=(pltpu.VMEM((64, 64), BF16), pltpu.VMEM(...  60 us
    unnamed x2, local copies, waits for them, and re-layouts  1.93 us

profile of v4, /device:TPU:1, one launch (start us, length us, event | category | flops | bytes accessed | tf_op | source)
XLA Modules:
  0.0 62.6 jit_solution(9383339754605508427)
XLA Ops:
  0.6 60.0 %layer_step.1 = (bf16[64,64]{1,0:T(8,128)(2,1)S(1)}, f32[2,8,128,256]{3,2,1,0:T(8,128)S(1)}) custom-call(bf16[64,64]{1,0:T(8,128)(2,1)} %tok_h.1, bf16[8,4,4096]{2,1,0:T(4,128)(2,1)} %bitcast.17, bf16[8,4,4096]{2,1,0:T(4,128)(2,1)} %bitcast.18, bf16[8,4,4096]{2,1,0:T(4,128)(2,1)} %bitcast.19, bf16[64,4096]{1,0:T(8,128)(2,1)} %bitcast.14, ...), custom_call_target="tpu_custom_call" | custom-call | tf_op jit(solution)/shard_map/layer_step/pallas_call | solution.py:483
  60.7 0.6 copy.20
  61.3 1.3 %copy.21 = f32[2,8,128,256]{3,2,1,0:T(8,128)} copy(f32[2,8,128,256]{3,2,1,0:T(8,128)S(1)} %get-tuple-element.3) | data formatting | bytes 4194304

commit v5 on v4

--- a/solution.py
+++ b/solution.py
@@ -40,7 +40,7 @@
     out, new_states,
     tok, bias, head_gain, g1, b1, g2, b2, wst, wc, owc, upc, dnc, st,
     s_a, r_a, s_g, r_g, x, s_b, r_b, ro, s_c, r_c, att32, att,
-    s_e, r_e, s_m, r_m, xt, xn, s_y, r_y, s_h, r_h, s_f, r_f, sq,
+    s_e, r_e, s_m, r_m, gain1, bias1, gm, s_y, r_y, s_h, r_h, s_f, r_f, sq,
     small_sem, own_sem, w_send, w_recv,
     az_send, az_recv, ax_send, ax_recv, g_sem, p_sem, b_sem, c_send, c_recv, e_send, e_recv, m_sem, y_sem, h_sem, f_sem,
 ):
@@ -249,6 +249,10 @@
 
     slot_c = t * 16 + lax.rem(kv, 16)
 
+    drain(r_g.at[t, pl.ds(0, 31)], g_sem.at[1])
+    gains = rcopy(r_g.at[t], r_g.at[t], p_sem, kv, partner)
+    gains.start()
+
     def send_c(src, slot, kv_to, t_to):
         pltpu.make_async_remote_copy(
             src_ref=src, dst_ref=r_c.at[slot], send_sem=c_send, recv_sem=c_recv.at[slot],
@@ -277,9 +281,24 @@
                 for e in (2, 1, 3):
                     send_c(r_c.at[slot], slot, z * 4 + xd[e], t)
 
-    drain(r_g.at[t, pl.ds(0, 31)], g_sem.at[1])
-    gains = rcopy(r_g.at[t], r_g.at[t], p_sem, kv, partner)
-    gains.start()
+    gains.wait()
+    ga = r_g[0, :, 0, :]
+    gb = r_g[1, :, 0, :]
+    lane32 = iota((32, 128), 1) < 64
+    gain1[...] = jnp.where(lane32, ga, pltpu.roll(gb, 64, 1))
+    bias1[...] = jnp.where(lane32, pltpu.roll(ga, 64, 1), gb)
+    wcopies[2].wait()
+    shift = [jnp.zeros((1, 256), F32) for _ in range(2)]
+    for c in range(CHIPS):
+        parts = []
+        for v in (gain1[c : c + 1, :], bias1[c : c + 1, :]):
+            high = v.astype(BF16).astype(F32)
+            parts += [high, v - high]
+        parts = jnp.concatenate(parts + [jnp.zeros((4, 128), F32)], axis=0).astype(BF16)
+        for tt in range(2):
+            r = dot(parts, upc[tt, c * 128 : (c + 1) * 128, :], NN)
+            gm[tt, c : c + 1, :] = r[0:1] + r[1:2]
+            shift[tt] = shift[tt] + (r[2:3] + r[3:4])
 
     for d in range(8):
         for e in range(4):
@@ -334,36 +353,38 @@
             send_e(r_e.at[slot], slot, z * 4 + xd[e])
     r_e[kv] = s_e[...]
     r_m[kv] = s_m[...]
-    gains.wait()
-    ga = r_g[0, :, 0, :]
-    gb = r_g[1, :, 0, :]
-    lane32 = iota((32, 128), 1) < 64
-    gain1 = jnp.where(lane32, ga, pltpu.roll(gb, 64, 1))
-    bias1 = jnp.where(lane32, pltpu.roll(ga, 64, 1), gb)
-    wcopies[2].wait()
-    wcopies[3].wait()
+    raw = [jnp.zeros((32, 256), F32) for _ in range(2)]
+    acc = jnp.zeros((32, 128), F32)
+    for d in (0, 1, 7, 2, 6, 3, 5, 4):
+        tiles = []
+        for e in range(1, 4):
+            drain(s_e, e_recv.at[zd[d] * 4 + xd[e]])
+        for j in range(4):
+            v = r_e[zd[d] * 4 + j].astype(F32)
+            acc = acc + v
+            tiles.append((v * gain1[pl.ds(zd[d] * 4 + j, 1), :]).astype(BF16))
+        tile = jnp.concatenate(tiles, axis=1)
+        for tt in range(2):
+            raw[tt] = raw[tt] + dot(tile, upc[tt, pl.ds(pl.multiple_of(zd[d] * 512, 512), 512), :], NN)
     drain(r_m.at[pl.ds(0, 31)], m_sem.at[1])
-    for d, e in FAR:
-        if e or d not in NEAR:
-            drain(s_e, e_recv.at[zd[d] * 4 + xd[e]])
     sq[0:32, :] = r_m[:, 0, :]
     means = sq[...].T[0:32, 0:32]
+    mean = (jnp.sum(acc, axis=-1, keepdims=True) + 128.0 * jnp.sum(means, axis=-1, keepdims=True)) / D
+    means = means - mean
     acc = jnp.zeros((32, 128), F32)
     for c in range(CHIPS):
-        acc = acc + r_e[c].astype(F32)
-    mean = (jnp.sum(acc, axis=-1, keepdims=True) + 128.0 * jnp.sum(means, axis=-1, keepdims=True)) / D
-    acc = jnp.zeros((32, 128), F32)
-    for c in range(CHIPS):
-        v = r_e[c].astype(F32) + (means[:, c : c + 1] - mean)
-        xt[c] = v
+        v = r_e[c].astype(F32) + means[:, c : c + 1]
         acc = acc + v * v
     inv = lax.rsqrt(jnp.sum(acc, axis=-1, keepdims=True) / D + LN_EPS)
-    for c in range(CHIPS):
-        xn[:, c * 128 : (c + 1) * 128] = (xt[c] * inv * gain1[c : c + 1, :] + bias1[c : c + 1, :]).astype(BF16)
-
+    own_gain = gain1[pl.ds(kv, 1), :]
+    own_bias = bias1[pl.ds(kv, 1), :]
+    normed = ((s_e[...].astype(F32) + (m_own - mean)) * inv * own_gain + own_bias).astype(BF16)
+
+    wcopies[3].wait()
     hidden = []
     for tt in range(2):
-        lifted = jnp.maximum(dot(xn[...], upc[tt], NN), 0.0)
+        level = lax.dot_general(means, gm[tt], NN, precision=lax.Precision.HIGHEST, preferred_element_type=F32)
+        lifted = jnp.maximum((raw[tt] + level) * inv + shift[tt], 0.0)
         hidden.append((lifted * lifted).astype(BF16))
     for d in (4, 3, 5, 2, 6, 1, 7, 0):
         cl = pl.ds(pl.multiple_of(zd[d] * 512, 512), 512)
@@ -377,7 +398,7 @@
 
     r_y[kv] = s_y[kv]
     drain(r_y.at[pl.ds(0, 31)], y_sem.at[1])
-    res2 = ALPHA * xn[:, pl.ds(at_chip, 128)].astype(F32)
+    res2 = ALPHA * normed.astype(F32)
     for c in range(CHIPS):
         res2 = res2 + r_y[c].astype(F32)
 
@@ -472,7 +493,7 @@
         V((2, 256, 128), F32), V((32, D), BF16),
         V((32, 128), BF16), V((32, 32, 128), BF16),
         V((1, 128), F32), V((32, 1, 128), F32),
-        V((32, 32, 128), F32), V((32, D), BF16),
+        V((32, 128), F32), V((32, 128), F32), V((2, 32, 256), F32),
         V((32, 32, 128), BF16), V((32, 32, 128), BF16),
         V((1, 128), F32), V((64, 1, 128), F32),
         V((32, 128), F32), V((32, 128), F32),

time: 62.7 us -> 62.2 us (level)
  no operation moved by 1% of the time
where the time goes in v5:
time: 62.2 us; the launch traced here: 62.1 us
  Pallas kernels  59.5 us (96%)
  local copies, waits for them, and re-layouts  1.93 us (3%)
  between operations  0.65 us (1%)
    pallas_call x1, Pallas kernels, body(): pl.pallas_call(kernel, out_shape=(pltpu.VMEM((64, 64), BF16), pltpu.VMEM(...  59.5 us
    unnamed x2, local copies, waits for them, and re-layouts  1.93 us

profile of v5, /device:TPU:1, one launch (start us, length us, event | category | flops | bytes accessed | tf_op | source)
XLA Modules:
  0.0 62.1 jit_solution(545187039032722516)
XLA Ops:
  0.6 59.5 %layer_step.1 = (bf16[64,64]{1,0:T(8,128)(2,1)S(1)}, f32[2,8,128,256]{3,2,1,0:T(8,128)S(1)}) custom-call(bf16[64,64]{1,0:T(8,128)(2,1)} %tok_h.1, bf16[8,4,4096]{2,1,0:T(4,128)(2,1)} %bitcast.17, bf16[8,4,4096]{2,1,0:T(4,128)(2,1)} %bitcast.18, bf16[8,4,4096]{2,1,0:T(4,128)(2,1)} %bitcast.19, bf16[64,4096]{1,0:T(8,128)(2,1)} %bitcast.14, ...), custom_call_target="tpu_custom_call" | custom-call | tf_op jit(solution)/shard_map/layer_step/pallas_call | solution.py:504
  60.2 0.6 copy.20
  60.8 1.3 %copy.21 = f32[2,8,128,256]{3,2,1,0:T(8,128)} copy(f32[2,8,128,256]{3,2,1,0:T(8,128)S(1)} %get-tuple-element.3) | data formatting | bytes 4194304

commit v6 on v5

--- a/solution.py
+++ b/solution.py
@@ -191,7 +191,7 @@
         p = projected[tt].astype(BF16)
         p = dot(p, perm, NN)
         for i in range(16):
-            s_b[i, tt] = p[2 * i : 2 * i + 2, :]
+            s_b[i, tt] = p[2 * i : 2 * i + 2, :].astype(BF16)
 
     for i in range(4):
         zl = wrap(z - 4 * half + i, 4)
@@ -225,8 +225,9 @@
         drain(r_b, b_sem.at[1])
 
     qkd, vg = [], []
+    arrived = r_b[...].astype(F32)
     for s in range(2):
-        rs = r_b[:, s, :]
+        rs = arrived[:, s, :]
         qkd.append(jnp.concatenate([rs[:, c * 32 : (c + 1) * 32] for c in range(4)], axis=0))
         vg.append(jnp.concatenate([rs[:, 128 + c * 16 : 144 + c * 16] for c in range(8)], axis=0))
     cols = dot(e1, jnp.concatenate(qkd, axis=1).astype(BF16), NN)
@@ -487,7 +488,7 @@
         V((2, 16, 128), BF16), V((64, 16, 128), BF16),
         V((2, 128), F32), V((2, 32, 2, 128), F32),
         V((32, D), BF16),
-        V((16, 2, 2, 256), F32), V((32, 2, 256), F32),
+        V((16, 2, 2, 256), BF16), V((32, 2, 256), BF16),
         V((16, 256), F32),
         V((16, 256), BF16), V((32, 16, 256), BF16),
         V((2, 256, 128), F32), V((32, D), BF16),

time: 62.2 us -> 61.7 us (level)
  no operation moved by 1% of the time
where the time goes in v6:
time: 61.7 us; the launch traced here: 61.6 us
  Pallas kernels  59.1 us (96%)
  local copies, waits for them, and re-layouts  1.93 us (3%)
  between operations  0.65 us (1%)
    pallas_call x1, Pallas kernels, body(): pl.pallas_call(kernel, out_shape=(pltpu.VMEM((64, 64), BF16), pltpu.VMEM(...  59.1 us
    unnamed x2, local copies, waits for them, and re-layouts  1.93 us

profile of v6, /device:TPU:1, one launch (start us, length us, event | category | flops | bytes accessed | tf_op | source)
XLA Modules:
  0.0 61.6 jit_solution(10124933271908711556)
XLA Ops:
  0.6 59.1 %layer_step.1 = (bf16[64,64]{1,0:T(8,128)(2,1)S(1)}, f32[2,8,128,256]{3,2,1,0:T(8,128)S(1)}) custom-call(bf16[64,64]{1,0:T(8,128)(2,1)} %tok_h.1, bf16[8,4,4096]{2,1,0:T(4,128)(2,1)} %bitcast.17, bf16[8,4,4096]{2,1,0:T(4,128)(2,1)} %bitcast.18, bf16[8,4,4096]{2,1,0:T(4,128)(2,1)} %bitcast.19, bf16[64,4096]{1,0:T(8,128)(2,1)} %bitcast.14, ...), custom_call_target="tpu_custom_call" | custom-call | tf_op jit(solution)/shard_map/layer_step/pallas_call | solution.py:505
  59.7 0.6 copy.20
  60.3 1.3 %copy.21 = f32[2,8,128,256]{3,2,1,0:T(8,128)} copy(f32[2,8,128,256]{3,2,1,0:T(8,128)S(1)} %get-tuple-element.3) | data formatting | bytes 4194304

commit v7 on v6

--- a/solution.py
+++ b/solution.py
@@ -193,7 +193,7 @@
         for i in range(16):
             s_b[i, tt] = p[2 * i : 2 * i + 2, :].astype(BF16)
 
-    for i in range(4):
+    for i in (2, 1, 3, 0):
         zl = wrap(z - 4 * half + i, 4)
         for j in (2, 1, 3, 0):
             k16 = zl * 4 + xd[j]
@@ -331,9 +331,6 @@
     res1 = ALPHA * x[:, pl.ds(at_chip, 128)].astype(F32) + mixed
 
     m_own = jnp.mean(res1, axis=-1, keepdims=True)
-    sq[0:32, :] = jnp.broadcast_to(m_own, (32, 128))
-    sq[32:128, :] = jnp.zeros((96, 128), F32)
-    s_m[...] = sq[...].T[0:1, :]
     s_e[...] = (res1 - m_own).astype(BF16)
 
     def send_e(src, slot, kv_to):
@@ -345,6 +342,9 @@
     for d, e in FAR:
         if e == 0 or d not in NEAR:
             send_e(s_e, kv, zd[d] * 4 + xd[e])
+    sq[0:32, :] = jnp.broadcast_to(m_own, (32, 128))
+    sq[32:128, :] = jnp.zeros((96, 128), F32)
+    s_m[...] = sq[...].T[0:1, :]
     for d, e in FAR:
         rcopy(s_m, r_m.at[kv], m_sem, zd[d] * 4 + xd[e], t).start()
     for d in NEAR:

time: 61.7 us -> 61.9 us (level)
  no operation moved by 1% of the time
where the time goes in v7:
time: 61.9 us; the launch traced here: 61.8 us
  Pallas kernels  59.3 us (96%)
  local copies, waits for them, and re-layouts  1.93 us (3%)
  between operations  0.65 us (1%)
    pallas_call x1, Pallas kernels, body(): pl.pallas_call(kernel, out_shape=(pltpu.VMEM((64, 64), BF16), pltpu.VMEM(...  59.3 us
    unnamed x2, local copies, waits for them, and re-layouts  1.93 us

profile of v7, /device:TPU:1, one launch (start us, length us, event | category | flops | bytes accessed | tf_op | source)
XLA Modules:
  0.0 61.8 jit_solution(289510502369422505)
XLA Ops:
  0.6 59.3 %layer_step.1 = (bf16[64,64]{1,0:T(8,128)(2,1)S(1)}, f32[2,8,128,256]{3,2,1,0:T(8,128)S(1)}) custom-call(bf16[64,64]{1,0:T(8,128)(2,1)} %tok_h.1, bf16[8,4,4096]{2,1,0:T(4,128)(2,1)} %bitcast.17, bf16[8,4,4096]{2,1,0:T(4,128)(2,1)} %bitcast.18, bf16[8,4,4096]{2,1,0:T(4,128)(2,1)} %bitcast.19, bf16[64,4096]{1,0:T(8,128)(2,1)} %bitcast.14, ...), custom_call_target="tpu_custom_call" | custom-call | tf_op jit(solution)/shard_map/layer_step/pallas_call | solution.py:505
  59.9 0.6 copy.20
  60.5 1.3 %copy.21 = f32[2,8,128,256]{3,2,1,0:T(8,128)} copy(f32[2,8,128,256]{3,2,1,0:T(8,128)S(1)} %get-tuple-element.3) | data formatting | bytes 4194304
